TPU v7x, 256 devices: a whole 4x4x8 slice. The times are simulated.
256 devices in a mesh: sp: 32 (over z, x), tp: 8 (over y, core).
Axes of the slice: x: 4, y: 4, z: 8, core: 2. Of those that a mesh axis runs over, the one named last changes fastest.
Arguments:
- hidden_in: bfloat16 [12288, 2048], P('sp', 'tp'), may hold values from -6 to 6
- in_gain: float32 [2048], replicated, may hold values from 0.1 to 1.9
- receptance_weight: bfloat16 [2048, 1024], P(None, 'tp'), may hold values from -0.125 to 0.125
- key_weight: bfloat16 [2048, 1024], P(None, 'tp'), may hold values from -0.125 to 0.125
- value_weight: bfloat16 [2048, 1024], P(None, 'tp'), may hold values from -0.125 to 0.125
- decay_down: bfloat16 [2048, 128], replicated, may hold values from -0.125 to 0.125
- decay_up: bfloat16 [128, 1024], P(None, 'tp'), may hold values from -0.5 to 0.5
- decay_base: float32 [1024], P('tp'), may hold values from -14 to -2
- decay_shift: float32 [12288, 1024], P('sp', 'tp'), may hold values from -1 to 0
- learn_rate: float32 [1024], P('tp'), may hold values from 0 to 1
- query_pair: bfloat16 [2048, 8, 128], P(None, 'tp'), may hold values from -1 to 1
- key_pair: bfloat16 [2048, 8, 128], P(None, 'tp'), may hold values from -1 to 1
- value_pair: bfloat16 [2048, 8, 128], P(None, 'tp'), may hold values from -0.125 to 0.125
- mix_lambda: float32 [8], P('tp'), may hold values from 0.3 to 0.8
- out_recurrent: bfloat16 [1024, 2048], P('tp'), may hold values from -0.1875 to 0.1875
- out_attention: bfloat16 [1024, 2048], P('tp'), may hold values from -0.1875 to 0.1875
- out_gain: float32 [2048], replicated, may hold values from 0.1 to 1.9
Outputs:
- layer_out: bfloat16 [12288, 2048], P(('sp', 'tp'))
- log_sums: float32 [8, 2, 12288], P('tp', None, 'sp')
All inputs are finite; a program needn't handle non-finite values.
Results may differ from a plain program's by a relative error of at most 0.018.
Values may be sent and summed in bfloat16 or wider, within the bound.
A program may use at most 128 MiB of HBM per device.

v0:
```python
import math

import jax
import jax.numpy as jnp
from jax import lax
from jax.sharding import Mesh
from jax.sharding import PartitionSpec as P

HD = 64
SP = ("sp_0", "sp_1")
SP_TP = ("sp_0", "sp_1", "tp")


HIGHEST = lax.Precision.HIGHEST
DECAY_SCALE = math.exp(-0.5)
NORM_EPS = 1e-06
GROUP_EPS = 0.00064
HEAD_EPS = 1e-05
KEY_EPS = 1e-06
NEGATIVE = -1e30
span_rows = 32
key_block = 1024


def in_one_piece(arrays, axis, dim, along):
    ends, at = ([], 0)
    for a in arrays[:-1]:
        at += a.shape[along]
        ends.append(at)
    both = jnp.concatenate(arrays, axis=along)
    return tuple(jnp.split(lax.all_gather(both, axis, axis=dim, tiled=True), ends, axis=along))


def copy_for_each(x, axis):
    copies = jnp.broadcast_to(x, (lax.axis_size(axis), *x.shape))
    return lax.all_to_all(copies, axis, split_axis=0, concat_axis=0, tiled=True)


def in_order(parts, dim):
    lengths = list(parts.shape[1:])
    lengths[dim] *= parts.shape[0]
    return jnp.moveaxis(parts, 0, dim).reshape(lengths)


def gather_directly(x, axis, dim):
    parts = copy_for_each(x, axis)
    return in_order(parts, dim)


def filled_with(x, identity):
    return jax.tree.map(
        lambda part, zero: jnp.zeros_like(part) + jnp.asarray(zero, part.dtype), x, identity
    )


def all_in_one(x, axis):
    leaves = jax.tree.leaves(x)
    order = sorted(range(len(leaves)), key=lambda k: -leaves[k].size)
    width = (1, *leaves[order[0]].shape)[-1]
    lines = [
        jnp.pad(leaves[k].reshape(-1), (0, -leaves[k].size % width)).reshape(-1, width)
        for k in order
    ]
    both, at, found = (lax.all_gather(jnp.concatenate(lines), axis), 0, {})
    for k, line in zip(order, lines):
        share = both[:, at : at + len(line)].reshape(len(both), -1)
        found[k] = share[:, : leaves[k].size].reshape(-1, *leaves[k].shape)
        at += len(line)
    numbers = iter(range(len(leaves)))
    return jax.tree.map(lambda _: found[next(numbers)], x)


def prefix_by_axis(x, axes, combine, identity):
    before = start = filled_with(x, identity)
    running = x
    for axis in reversed(axes):
        devices, mine = (lax.axis_size(axis), lax.axis_index(axis))
        pieces = all_in_one(
            jax.tree.map(
                lambda part, kind: part.astype(kind),
                running,
                jax.tree.map(lambda a: jnp.bfloat16 if a.dtype == jnp.float32 else a.dtype, x),
            ),
            axis,
        )
        inside, running = (start, start)
        for k in range(devices):
            passed = k < mine
            running = combine(
                running, jax.tree.map(lambda part, own: part[k].astype(own.dtype), pieces, x)
            )
            inside = jax.tree.map(lambda new, old: jnp.where(passed, new, old), running, inside)
        before = combine(inside, before)
    return before


def cut_along(x, dim, devices):
    before, after = (x.shape[:dim], x.shape[dim + 1 :])
    return jnp.moveaxis(x.reshape(*before, devices, -1, *after), dim, 0)


def sent_and_summed(x, axis, dim):
    devices = lax.axis_size(axis)
    parts = lax.all_to_all(cut_along(x, dim, devices), axis, 0, 0, tiled=True)
    return jnp.sum(parts.astype(jnp.float32), axis=0)


def rms_rows(values, gain):
    wide = values.astype(jnp.float32)
    return wide * lax.rsqrt(jnp.mean(wide * wide, axis=-1, keepdims=True) + NORM_EPS) * gain


def project(normed, weight):
    return jnp.dot(
        normed, weight.reshape(weight.shape[0], -1), preferred_element_type=jnp.float32
    ).astype(jnp.bfloat16)


def compose(earlier, later):
    return (
        jnp.einsum("...ij,...jk->...ik", earlier[0], later[0], precision=HIGHEST),
        jnp.einsum("...ij,...jk->...ik", earlier[1], later[0], precision=HIGHEST) + later[1],
    )


def by_blocks(values, head_count):
    block_total = values.shape[0] // span_rows
    return (
        values.astype(jnp.float32)
        .reshape(block_total, span_rows, head_count, HD)
        .transpose(0, 2, 1, 3)
    )


def product(left, right):
    return jnp.einsum("bhts,bhsv->bhtv", left, right, precision=HIGHEST)


def block_terms(receptance, key_rows, value_rows, log_decay, learning):
    running = jnp.cumsum(log_decay, axis=2)
    before = running - log_decay
    middle = running[:, :, span_rows // 2 - 1 : span_rows // 2, :]
    ending = running[:, :, span_rows - 1 :, :]
    unit_keys = key_rows * lax.rsqrt(jnp.sum(key_rows * key_rows, axis=-1, keepdims=True) + KEY_EPS)
    erasing = unit_keys * learning
    against = -unit_keys
    against_scaled = against * jnp.exp(before - middle)
    read_scaled = receptance * jnp.exp(running - middle)
    erase_scaled = erasing * jnp.exp(middle - running)
    keys_scaled = key_rows * jnp.exp(middle - running)
    strict = jnp.tril(jnp.ones((span_rows, span_rows), jnp.float32), -1)
    causal = jnp.tril(jnp.ones((span_rows, span_rows), jnp.float32))

    def pair_scores(left, right, keep_mask):
        return jnp.einsum("bhtk,bhsk->bhts", left, right, precision=HIGHEST) * keep_mask

    lower_part = pair_scores(against_scaled, erase_scaled, strict)
    carry_keys = pair_scores(against_scaled, keys_scaled, strict)
    read_erase = pair_scores(read_scaled, erase_scaled, causal)
    read_keys = pair_scores(read_scaled, keys_scaled, causal)
    right_side = jnp.concatenate(
        [against * jnp.exp(before), product(carry_keys, value_rows)], axis=-1
    )
    identity = jnp.eye(span_rows, dtype=jnp.float32)
    solved = lax.linalg.triangular_solve(
        identity - lower_part, right_side, left_side=True, lower=True, unit_diagonal=True
    )
    from_state = solved[..., :HD]
    from_values = solved[..., HD:]
    to_end = jnp.exp(ending - running)
    erase_end = erasing * to_end
    keys_end = key_rows * to_end
    transfer = jnp.eye(HD, dtype=jnp.float32) * jnp.exp(ending) + jnp.einsum(
        "bhsk,bhsj->bhkj", from_state, erase_end, precision=HIGHEST
    )
    added = jnp.einsum("bhsv,bhsk->bhvk", from_values, erase_end, precision=HIGHEST) + jnp.einsum(
        "bhsv,bhsk->bhvk", value_rows, keys_end, precision=HIGHEST
    )
    read_state = receptance * jnp.exp(running) + product(read_erase, from_state)
    local_read = product(read_erase, from_values) + product(read_keys, value_rows)
    return (transfer, added, read_state, local_read)


def recurrent_terms(
    normed,
    receptance_weight,
    key_weight,
    value_weight,
    decay_down,
    decay_up,
    decay_base,
    decay_shift,
    learn_rate,
):
    head_count = receptance_weight.shape[1] // HD
    receptance = project(normed, receptance_weight)
    key_rows = project(normed, key_weight)
    value_rows = project(normed, value_weight)
    low_rank = jnp.tanh(jnp.dot(normed, decay_down, preferred_element_type=jnp.float32)).astype(
        jnp.bfloat16
    )
    log_decay = (
        -DECAY_SCALE
        * jax.nn.sigmoid(
            jnp.dot(low_rank, decay_up, preferred_element_type=jnp.float32) + decay_base
        )
        + decay_shift
    )
    learning = learn_rate.reshape(1, head_count, 1, HD)
    return block_terms(
        by_blocks(receptance, head_count),
        by_blocks(key_rows, head_count),
        by_blocks(value_rows, head_count),
        by_blocks(log_decay, head_count),
        learning,
    )


def attention_branch(normed, query_pair, key_pair, value_pair, mix_lambda, position_base):
    row_count = normed.shape[0]
    head_count = mix_lambda.shape[0]
    queries = project(normed, query_pair).reshape(row_count, head_count, 2, HD)
    pair_keys = project(normed, key_pair).reshape(row_count, head_count, 2 * HD)
    pair_values = project(normed, value_pair).reshape(row_count, head_count, 2 * HD)
    score_scale = HD ** (-0.5)
    query_places = position_base + jnp.arange(row_count)

    def one_block(carried, key_part, value_part, offset):
        row_max, row_sum, weighted = carried
        length = key_part.shape[0]
        scores = (
            jnp.einsum(
                "qhmd,khmd->hmqk",
                queries,
                key_part.reshape(length, head_count, 2, HD),
                preferred_element_type=jnp.float32,
            )
            * score_scale
        )
        allowed = query_places[:, None] >= (offset + jnp.arange(length))[None, :]
        scores = jnp.where(allowed, scores, NEGATIVE)
        new_max = jnp.maximum(row_max, jnp.max(scores, axis=-1))
        rescale = jnp.exp(row_max - new_max)
        weights = jnp.where(allowed, jnp.exp(scores - new_max[..., None]), 0.0)
        row_sum = row_sum * rescale + jnp.sum(weights, axis=-1)
        weighted = weighted * rescale[..., None] + jnp.einsum(
            "hmqk,khv->hmqv",
            weights.astype(jnp.bfloat16),
            value_part,
            preferred_element_type=jnp.float32,
        )
        return (new_max, row_sum, weighted)

    initial = (
        jnp.full((head_count, 2, row_count), NEGATIVE, jnp.float32),
        jnp.zeros((head_count, 2, row_count), jnp.float32),
        jnp.zeros((head_count, 2, row_count, 2 * HD), jnp.float32),
    )
    key_part, value_part = in_one_piece((pair_keys, pair_values), SP, 0, 1)
    length = key_part.shape[0]
    block_size = length
    while block_size > key_block and block_size % 2 == 0:
        block_size = block_size // 2
    block_total = length // block_size

    def compute(current):
        key_blocks = key_part.reshape(block_total, block_size, head_count, 2 * HD)
        value_blocks = value_part.reshape(block_total, block_size, head_count, 2 * HD)

        def scan_step(running_state, inputs):
            key_one, value_one, block_number = inputs
            return (one_block(running_state, key_one, value_one, block_number * block_size), 0)

        return lax.scan(scan_step, current, (key_blocks, value_blocks, jnp.arange(block_total)))[0]

    def keep_state(current):
        return current

    row_max, row_sum, weighted = lax.cond(
        jnp.int32(0) <= query_places[-1], compute, keep_state, initial
    )
    map_out = weighted / row_sum[..., None]
    head_out = map_out[:, 0] - mix_lambda[:, None, None] * map_out[:, 1]
    head_out = head_out * lax.rsqrt(
        jnp.mean(head_out * head_out, axis=-1, keepdims=True) + HEAD_EPS
    )
    att_mix = (
        head_out.transpose(1, 0, 2).reshape(row_count, head_count * 2 * HD).astype(jnp.bfloat16)
    )
    return (att_mix, row_max + jnp.log(row_sum))


def per_device(
    hidden_in,
    in_gain,
    receptance_weight,
    key_weight,
    value_weight,
    decay_down,
    decay_up,
    decay_base,
    decay_shift,
    learn_rate,
    query_pair,
    key_pair,
    value_pair,
    mix_lambda,
    out_recurrent,
    out_attention,
    out_gain,
):
    whole_rows = gather_directly(hidden_in, "tp", 1)
    normed = rms_rows(whole_rows, in_gain).astype(jnp.bfloat16)
    row_count = normed.shape[0]
    head_count = receptance_weight.shape[1] // HD
    transfer, added, read_state, local_read = recurrent_terms(
        normed,
        receptance_weight,
        key_weight,
        value_weight,
        decay_down,
        decay_up,
        decay_base,
        decay_shift,
        learn_rate,
    )
    inclusive = lax.associative_scan(compose, (transfer, added), axis=0)
    device_total = (inclusive[0][-1], inclusive[1][-1])
    identity = jnp.broadcast_to(jnp.eye(HD, dtype=jnp.float32), (head_count, HD, HD))
    earlier = prefix_by_axis(device_total, SP, compose, (identity, jnp.zeros_like(identity)))
    state_in = earlier[1]
    block_map = jnp.concatenate([identity[None], inclusive[0][:-1]], axis=0)
    block_add = jnp.concatenate([jnp.zeros_like(identity)[None], inclusive[1][:-1]], axis=0)
    start_state = jnp.einsum("hvk,bhkj->bhvj", state_in, block_map, precision=HIGHEST) + block_add
    recurrent = local_read + jnp.einsum(
        "bhtk,bhvk->bhtv", read_state, start_state, precision=HIGHEST
    )
    recurrent = recurrent.transpose(0, 2, 1, 3).reshape(row_count, head_count, HD)
    centered = recurrent - jnp.mean(recurrent, axis=-1, keepdims=True)
    rec_mix = centered * lax.rsqrt(
        jnp.mean(centered * centered, axis=-1, keepdims=True) + GROUP_EPS
    )
    rec_mix = rec_mix.reshape(row_count, head_count * HD).astype(jnp.bfloat16)
    position_base = lax.axis_index(SP) * row_count
    att_mix, log_sums = attention_branch(
        normed, query_pair, key_pair, value_pair, mix_lambda, position_base
    )
    projected = sent_and_summed(
        (
            jnp.dot(rec_mix, out_recurrent, preferred_element_type=jnp.float32)
            + jnp.dot(att_mix, out_attention, preferred_element_type=jnp.float32)
        ).astype(jnp.bfloat16),
        "tp",
        0,
    )
    layer_out = rms_rows(projected, out_gain).astype(jnp.bfloat16)
    return (layer_out, log_sums)


def solution(mesh):
    split = Mesh(mesh.devices.reshape(8, 4, mesh.shape["tp"]), ("sp_0", "sp_1", "tp"))
    placed = (
        P(SP, "tp"),
        P(),
        P(None, "tp"),
        P(None, "tp"),
        P(None, "tp"),
        P(),
        P(None, "tp"),
        P("tp"),
        P(SP, "tp"),
        P("tp"),
        P(None, "tp", None),
        P(None, "tp", None),
        P(None, "tp", None),
        P("tp"),
        P("tp", None),
        P("tp", None),
        P(),
    )
    return jax.shard_map(
        per_device,
        mesh=split,
        in_specs=placed,
        out_specs=(P(SP_TP, None), P("tp", None, SP)),
        check_vma=False,
    )
```

profile of v0, /device:TPU:1, one launch (start us, length us, event | category | flops | bytes accessed | tf_op | source)
XLA Modules:
  0.0 463.6 jit_solution(13114811459258641148)
XLA Ops:
  9.7 6.7 %all-to-all-start = ((bf16[8,384,256]{1,2,0:T(8,128)(2,1)}), bf16[8,384,256]{1,2,0:T(8,128)(2,1)S(1)}, u32[]{:S(2)}, u32[]{:S(2)}) async-start(bf16[8,384,256]{1,2,0:T(8,128)(2,1)} %broadcast_in_dim.72), calls=%async_computation | async-start | bytes 3145728 | tf_op jit(solution)/shard_map/all_to_all | solution.py:36
  19.7 17.2 %all-to-all-done = bf16[8,384,256]{1,2,0:T(8,128)(2,1)S(1)} async-done(((bf16[8,384,256]{1,2,0:T(8,128)(2,1)}), bf16[8,384,256]{1,2,0:T(8,128)(2,1)S(1)}, u32[]{:S(2)}, u32[]{:S(2)}) %all-to-all-start) | async-done | bytes 1572896 | tf_op jit(solution)/shard_map/all_to_all | solution.py:36
  38.2 1.8 fusion.19
  43.0 1.8 fusion.31
  48.5 59.8 %custom-call.3 = f32[12,2,1,32,32]{3,4,2,1,0:T(8,128)} custom-call(f32[12,2,1,32,32]{4,3,2,1,0:T(8,128)S(1)} %fusion.25), custom_call_target="InvertDiagBlocksLowerTriangular" | custom-call | tf_op jit(solution)/shard_map/triangular_solve | solution.py:165
  112.7 2.4 convolution_add_fusion
  122.5 3.4 pad.45
  127.5 4.3 pad.48
  134.7 4.3 pad.47
  138.9 1.9 add.259
  140.8 7.1 %pad.50 = f32[12,2,64,64]{3,2,1,0:T(8,128)} pad(f32[6,2,64,64]{3,2,1,0:T(8,128)} %add.259, f32[]{:T(128)} %constant.49.clone.1), padding=1_0_1x0_0_0x0_0_0x0_0_0 | pad | bytes 589828 | tf_op jit(solution)/shard_map/pad | solution.py:327
  150.4 7.1 %pad.75 = f32[11,2,64,64]{3,2,1,0:T(8,128)} pad(f32[6,2,64,64]{3,2,1,0:T(8,128)} %pad_maximum_fusion.1, f32[]{:T(128)} %constant.49.clone.1), padding=0_0_1x0_0_0x0_0_0x0_0_0 | pad | bytes 557060 | tf_op jit(solution)/shard_map/slice | solution.py:333
  157.5 7.1 %pad.49 = f32[12,2,64,64]{3,2,1,0:T(8,128)} pad(f32[6,2,64,64]{3,2,1,0:T(8,128)} %pad_maximum_fusion.1, f32[]{:T(128)} %constant.49.clone.1), padding=0_1_1x0_0_0x0_0_0x0_0_0 | pad | bytes 589828 | tf_op jit(solution)/shard_map/pad | solution.py:327
  168.8 3.4 pad.39
  173.9 4.3 pad.42
  180.1 4.3 pad.41
  184.4 2.0 add.250
  186.4 7.2 %pad.114 = f32[11,2,64,64]{3,2,1,0:T(8,128)} pad(f32[6,2,64,64]{3,2,1,0:T(8,128)} %add.250, f32[]{:T(128)} %constant.49.clone.1), padding=0_0_1x0_0_0x0_0_0x0_0_0 | pad | bytes 557060
  193.5 7.1 %pad.44 = f32[12,2,64,64]{3,2,1,0:T(8,128)} pad(f32[6,2,64,64]{3,2,1,0:T(8,128)} %add.250, f32[]{:T(128)} %constant.49.clone.1), padding=1_0_1x0_0_0x0_0_0x0_0_0 | pad | bytes 589828 | tf_op jit(solution)/shard_map/pad | solution.py:327
  200.7 2.9 fusion.34
  203.5 1.9 reshape.443
  207.8 7.1 %pad.43 = f32[12,2,64,64]{3,2,1,0:T(8,128)} pad(f32[6,2,64,64]{3,2,1,0:T(8,128)} %pad_maximum_fusion, f32[]{:T(128)} %constant.49.clone.1), padding=0_1_1x0_0_0x0_0_0x0_0_0 | pad | bytes 589828 | tf_op jit(solution)/shard_map/pad | solution.py:327
  216.7 9.7 %all-gather = bf16[1024,64]{1,0:T(8,128)(2,1)S(1)} all-gather(bf16[256,64]{1,0:T(8,128)(2,1)S(1)} %pad_maximum_fusion.7), channel_id=2, replica_groups=mesh['sp_0'=8,'sp_1'=4,'tp'=8] {'sp_1'}, dimensions={0}, use_global_device_ids=true | all-gather | bytes 163840 | tf_op jit(solution)/shard_map/all_gather | solution.py:64
  227.8 23.2 %all-gather.1 = bf16[2048,64]{1,0:T(8,128)(2,1)S(1)} all-gather(bf16[256,64]{1,0:T(8,128)(2,1)S(1)} %pad_maximum_fusion.8), channel_id=3, replica_groups=mesh['sp_0'=8,'sp_1'=4,'tp'=8] {'sp_0'}, dimensions={0}, use_global_device_ids=true | all-gather | bytes 294912 | tf_op jit(solution)/shard_map/all_gather | solution.py:64
  260.3 1.7 convolution_convert_fusion
  262.0 2.3 fusion.93
  264.3 153.1 %conditional.1 = (f32[1,2,384]{2,1,0:T(2,128)}, f32[1,2,384]{2,1,0:T(2,128)}, f32[1,2,384,128]{3,2,1,0:T(8,128)}, f32[1,2,384]{2,1,0:T(2,128)S(1)}) conditional(s32[]{:T(128)} %bitcast.59, () %tuple.20, (bf16[12288,2,128]{2,0,1:T(8,128)(2,1)}, bf16[384,128]{1,0:T(8,128)(2,1)S(1)}, s32[384]{0:T(512)S(1)}) %tuple.21), branch_computations={%region_5.6_spmd, %region_6.11_spmd} | conditional | flops 234755328 | bytes 23164788 | solution.py:279
  264.4 4.7 %fusion.140 = (bf16[12288,1,128]{2,0,1:T(8,128)(2,1)}, bf16[12288,1,128]{2,0,1:T(8,128)(2,1)}) fusion(bf16[12288,2,128]{2,0,1:T(8,128)(2,1)} %get-tuple-element.57), kind=kLoop, calls=%fused_computation.240 | loop fusion | bytes 12582912 | tf_op jit(solution)/shard_map/split | solution.py:31
  269.2 147.6 %while.14 = (s32[]{:T(128)}, f32[1,2,384]{2,1,0:T(2,128)}, f32[1,2,384]{2,1,0:T(2,128)}, f32[1,2,384,128]{3,2,1,0:T(8,128)}, s32[384]{0:T(512)S(1)}, /*index=5*/...) while((s32[]{:T(128)}, f32[1,2,384]{2,1,0:T(2,128)}, ...), condition=%wide.region_10.10_spmd.clone, body=%wide.region_7.9_spmd.clone.sunk | while | flops 234755328 | bytes 10378925 | solution.py:274
  273.1 2.6 fusion.220
  281.6 2.8 fusion.220
  290.9 2.8 fusion.220
  300.2 2.8 fusion.220
  309.6 2.8 fusion.220
  318.9 2.8 fusion.220
  328.2 2.8 fusion.220
  337.5 2.8 fusion.220
  346.8 2.8 fusion.220
  356.1 2.8 fusion.220
  365.5 2.8 fusion.220
  374.8 2.8 fusion.220
  384.1 2.8 fusion.220
  393.4 2.8 fusion.220
  402.7 2.8 fusion.220
  412.1 2.8 fusion.220
  418.8 3.7 add_convert_fusion
  422.5 12.5 %all-to-all-start.1 = ((bf16[8,48,2048]{2,1,0:T(8,128)(2,1)}), bf16[8,48,2048]{2,1,0:T(8,128)(2,1)S(1)}, u32[]{:S(2)}, u32[]{:S(2)}) async-start(bf16[8,48,2048]{2,1,0:T(8,128)(2,1)} %bitcast.306), calls=%async_computation.1 | async-start | bytes 3145728 | tf_op jit(solution)/shard_map/all_to_all | solution.py:104
  436.3 19.4 %all-to-all-done.1 = bf16[8,48,2048]{2,1,0:T(8,128)(2,1)S(1)} async-done(((bf16[8,48,2048]{2,1,0:T(8,128)(2,1)}), bf16[8,48,2048]{2,1,0:T(8,128)(2,1)S(1)}, u32[]{:S(2)}, u32[]{:S(2)}) %all-to-all-start.1) | async-done | bytes 1572896 | tf_op jit(solution)/shard_map/all_to_all | solution.py:104
  (368 shorter events, 148.7 us)
Async XLA Ops:
  7.2 254.8 %copy-start = (bf16[128,2048]{1,0:T(8,128)(2,1)S(1)}, bf16[128,2048]{1,0:T(8,128)(2,1)}, u32[]{:S(2)}) copy-start(bf16[128,2048]{1,0:T(8,128)(2,1)} %param.35) | copy-start | bytes 1572868
  8.3 8.7 %copy-start.36 = (f32[128]{0:T(128)S(1)}, f32[128]{0:T(128)}, u32[]{:S(2)}) copy-start(f32[128]{0:T(128)} %param.30) | copy-start | bytes 1540
  8.3 10.0 %copy-start.27 = (f32[2048]{0:T(1024)S(1)}, f32[2048]{0:T(1024)}, u32[]{:S(2)}) copy-start(f32[2048]{0:T(1024)} %param.22) | copy-start | bytes 24580
  9.7 27.3 %all-to-all-start = ((bf16[8,384,256]{1,2,0:T(8,128)(2,1)}), bf16[8,384,256]{1,2,0:T(8,128)(2,1)S(1)}, u32[]{:S(2)}, u32[]{:S(2)}) async-start(bf16[8,384,256]{1,2,0:T(8,128)(2,1)} %broadcast_in_dim.72), calls=%async_computation | async-start | bytes 3145728 | tf_op jit(solution)/shard_map/all_to_all | solution.py:36
  16.4 247.9 %all-gather.4.cloned.1.call-start = ((), (), s32[]{:S(2)}) async-start(), calls=%async_computation.2 | async-start | bytes 6488064 | tf_op jit(solution)/shard_map/all_gather | solution.py:31
  17.1 93.1 %copy-start.31 = (f32[2,64]{1,0:T(2,128)}, f32[2,64]{1,0:T(2,128)S(1)}, u32[]{:S(2)}) copy-start(f32[2,64]{1,0:T(2,128)S(1)} %mul.261) | copy-start | bytes 1540
  19.6 90.6 %copy-start.13 = (f32[64,64]{1,0:T(8,128)}, f32[64,64]{1,0:T(8,128)S(1)}, u32[]{:S(2)}) copy-start(f32[64,64]{1,0:T(8,128)S(1)} %fusion.121) | copy-start | bytes 49156
  19.7 20.3 %copy-start.20 = (bf16[2048,128]{1,0:T(8,128)(2,1)S(1)}, bf16[2048,128]{1,0:T(8,128)(2,1)}, u32[]{:S(2)}) copy-start(bf16[2048,128]{1,0:T(8,128)(2,1)} %param.25) | copy-start | bytes 1572868
  37.0 1.2 copy-start.2
  38.2 2.5 copy-start.29
  40.0 2.9 copy-start.1
  40.7 2.3 copy-start.34
  40.7 2.3 copy-start.35
  40.7 2.3 copy-start.37
  43.0 69.7 %copy-start.16 = (f32[12,2,32]{2,1,0:T(2,128)}, f32[12,2,32]{2,1,0:T(2,128)S(1)}, u32[]{:S(2)}) copy-start(f32[12,2,32]{2,1,0:T(2,128)S(1)} %add_rsqrt_fusion.1) | copy-start | bytes 9220
  48.5 61.7 %copy-start.26 = (f32[12,2,64]{2,1,0:T(2,128)S(1)}, f32[12,2,64]{2,1,0:T(2,128)}, u32[]{:S(2)}) copy-start(f32[12,2,64]{2,1,0:T(2,128)} %copy.71) | copy-start | bytes 18436
  108.3 1.0 copy-start.24
  111.8 3.4 copy-start.4
  112.3 4.0 copy-start.6
  112.7 4.7 %copy-start.12 = (f32[3,2,64,64]{3,2,1,0:T(8,128)}, f32[3,2,64,64]{3,2,1,0:T(8,128)S(1)}, u32[]{:S(2)}) copy-start(f32[3,2,64,64]{3,2,1,0:T(8,128)S(1)} %fusion.82) | copy-start | bytes 294916
  112.7 5.5 %copy-start.3 = (bf16[8,384,256]{1,2,0:T(8,128)(2,1)S(1)}, bf16[8,384,256]{1,2,0:T(8,128)(2,1)}, u32[]{:S(2)}) copy-start(bf16[8,384,256]{1,2,0:T(8,128)(2,1)} %copy-done.2) | copy-start | bytes 4718596
  112.7 5.5 %copy-start.28 = (f32[8,256]{1,0:T(8,128)S(1)}, f32[8,256]{1,0:T(8,128)}, u32[]{:S(2)}) copy-start(f32[8,256]{1,0:T(8,128)} %mul.289) | copy-start | bytes 24580
  112.7 5.5 %copy-start.30 = (f32[384]{0:T(512)S(1)}, f32[384]{0:T(512)}, u32[]{:S(2)}) copy-start(f32[384]{0:T(512)} %copy-done.29) | copy-start | bytes 4612
  115.1 3.0 copy-start.8
  115.7 2.5 copy-start.15
  115.7 2.9 copy-start.21
  116.7 1.5 copy-start.18
  118.2 1.1 copy-start.22
  119.3 2.5 slice-start.3
  133.1 16.5 %slice-start.2 = ((f32[12,2,64,64]{3,2,1,0:T(8,128)}), f32[1,2,64,64]{3,2,1,0:T(8,128)S(1)}, s32[]{:S(2)}) async-start(f32[12,2,64,64]{3,2,1,0:T(8,128)} %copy-done.8), calls=%async_computation.5 | async-start | bytes 131072 | tf_op jit(solution)/shard_map/slice | solution.py:327
  150.4 29.0 %slice-start.1 = ((f32[6,2,64,64]{3,2,1,0:T(8,128)}), f32[1,2,64,64]{3,2,1,0:T(8,128)S(1)}, s32[]{:S(2)}) async-start(f32[6,2,64,64]{3,2,1,0:T(8,128)} %copy-done.6), calls=%async_computation.4 | async-start | bytes 131072 | tf_op jit(solution)/shard_map/slice | solution.py:327
  165.7 0.6 copy-start.19
  200.7 6.3 %slice-start = ((f32[12,2,64,64]{3,2,1,0:T(8,128)}), f32[1,2,64,64]{3,2,1,0:T(8,128)S(1)}, s32[]{:S(2)}) async-start(f32[12,2,64,64]{3,2,1,0:T(8,128)} %copy-done.4), calls=%async_computation.3 | async-start | bytes 131072 | tf_op jit(solution)/shard_map/slice | solution.py:327
  207.8 18.6 %copy-start.14 = (f32[64,64]{1,0:T(8,128)S(1)}, f32[64,64]{1,0:T(8,128)}, u32[]{:S(2)}) copy-start(f32[64,64]{1,0:T(8,128)} %copy-done.13) | copy-start | bytes 49156
  227.8 25.3 %copy-start.7 = (f32[12,2,64,64]{3,2,1,0:T(8,128)S(1)}, f32[12,2,64,64]{3,2,1,0:T(8,128)}, u32[]{:S(2)}) copy-start(f32[12,2,64,64]{3,2,1,0:T(8,128)} %pad.50) | copy-start | bytes 1179652
  227.8 25.3 %copy-start.11 = (f32[11,2,64,64]{3,2,1,0:T(8,128)S(1)}, f32[11,2,64,64]{3,2,1,0:T(8,128)}, u32[]{:S(2)}) copy-start(f32[11,2,64,64]{3,2,1,0:T(8,128)} %pad.75) | copy-start | bytes 1081348
  251.4 1.8 copy-start.9
  251.4 1.8 copy-start.10
  253.2 1.1 copy-start.5
  253.2 1.1 copy-start.17
  253.2 1.1 copy-start.25
  253.2 1.1 copy-start.32
  264.3 154.5 %copy-start.23 = (bf16[128,2048]{1,0:T(8,128)(2,1)S(1)}, bf16[128,2048]{1,0:T(8,128)(2,1)}, u32[]{:S(2)}) copy-start(bf16[128,2048]{1,0:T(8,128)(2,1)} %param.36) | copy-start | bytes 1572868
  422.5 33.5 %copy-start.33 = (f32[2048]{0:T(1024)S(1)}, f32[2048]{0:T(1024)}, u32[]{:S(2)}) copy-start(f32[2048]{0:T(1024)} %param.37) | copy-start | bytes 24580
  422.5 33.2 %all-to-all-start.1 = ((bf16[8,48,2048]{2,1,0:T(8,128)(2,1)}), bf16[8,48,2048]{2,1,0:T(8,128)(2,1)S(1)}, u32[]{:S(2)}, u32[]{:S(2)}) async-start(bf16[8,48,2048]{2,1,0:T(8,128)(2,1)} %bitcast.306), calls=%async_computation.1 | async-start | bytes 3145728 | tf_op jit(solution)/shard_map/all_to_all | solution.py:104
Sparse Core Ops, SparseCore 0:
  120.8 87.7 all-gather.3
where the time goes:
time: 472 us; the launch traced here: 464 us
  other arithmetic  128 us (27%)
  local copies, waits for them, and re-layouts  121 us (26%)
  matrix products  97.9 us (21%)
  waiting for transfers between devices  36.6 us (8%)
  blocking collectives  32.9 us (7%)
  starting transfers between devices  19.2 us (4%)
  between operations  16.5 us (3%)
  loops' own time  11.5 us (2%)
    another operation x4, other arithmetic, block_terms(): lax.linalg.triangular_solve(identity - lower_part, right_side, left_side=...  59.9 us
    pad x10, local copies, waits for them, and re-layouts, per_device(): inclusive = lax.associative_scan(compose, (transfer, added), axis=0)  52.5 us
    dot_general x16, matrix products, one_block(): jnp.einsum('hmqk,khv->hmqv', weights.astype(jnp.bfloat16), value_part, pr...  44.5 us
    all_gather x2, blocking collectives, all_in_one(): both, at, found = (lax.all_gather(jnp.concatenate(lines), axis), 0, {})  32.9 us
    dynamic_slice x48, local copies, waits for them, and re-layouts, compute(): lax.scan(scan_step, current, (key_blocks, value_blocks, jnp.arange(block_...  28 us
    add x16, other arithmetic, one_block(): row_sum = row_sum * rescale + jnp.sum(weights, axis=-1)  20 us
    all_to_all x1, waiting for transfers between devices, sent_and_summed(): parts = lax.all_to_all(cut_along(x, dim, devices), axis, 0, 0, tiled=True)  19.4 us
    all_to_all x1, waiting for transfers between devices, copy_for_each(): return lax.all_to_all(copies, axis, split_axis=0, concat_axis=0, tiled=True)  17.2 us
  transfers between devices with their start and end apart: 3, of which 2 were waited for; matrix products, arithmetic and copies ran while one was open for 24% of the time, Pallas kernels for 0%

commit v1 on v0

v1 whole, which is shorter than its diff:
```python
import functools
import math

import jax
import jax.numpy as jnp
from jax import lax
from jax.experimental import pallas as pl
from jax.experimental.pallas import tpu as pltpu
from jax.sharding import Mesh
from jax.sharding import PartitionSpec as P

F32 = jnp.float32
BF16 = jnp.bfloat16
HD = 64
NZ, NX, NY, NC = 8, 4, 4, 2
ROWS = 384
HALF = ROWS // 2
D = 2048
FEAT = 256
CHUNK = 128
SUB = 32
DECAY_SCALE = math.exp(-0.5)
NORM_EPS = 1e-06
GROUP_EPS = 0.00064
HEAD_EPS = 1e-05
KEY_EPS = 1e-06
NEGATIVE = -1e30
TINY = 1e-37
LOG2E = 1.4426950408889634
LN2 = 0.6931471805599453
MESH = pl.DeviceIdType.MESH
VMEM = pltpu.VMEM
HIGHEST = lax.Precision.HIGHEST


def dot(a, b):
    return jnp.dot(a, b, preferred_element_type=F32)


def dot_nt(a, b):
    return lax.dot_general(a, b, (((1,), (1,)), ((), ())), preferred_element_type=F32)


def split(x):
    high = x.astype(BF16)
    return high, (x - high.astype(F32)).astype(BF16)


def fine_dot(a, b):
    a_high, a_low = split(a)
    b_high, b_low = split(b)
    both = dot(jnp.concatenate([a_high, a_low], 1), jnp.concatenate([b_high, b_high], 0))
    return both + dot(a_high, b_low)


def fine_dot_nt(a, b):
    a_high, a_low = split(a)
    b_high, b_low = split(b)
    both = dot_nt(jnp.concatenate([a_high, a_low], 1), jnp.concatenate([b_high, b_high], 1))
    return both + dot_nt(a_high, b_low)


def coarse_dot(a, b):
    return dot(a.astype(BF16), b.astype(BF16))


def remote(src, dst, send_sem, recv_sem, where):
    return pltpu.make_async_remote_copy(
        src_ref=src,
        dst_ref=dst,
        send_sem=send_sem,
        recv_sem=recv_sem,
        device_id=where,
        device_id_type=MESH,
    )


def greet(places):
    barrier = pltpu.get_barrier_semaphore()
    for place in places:
        pl.semaphore_signal(barrier, inc=1, device_id=place, device_id_type=MESH)
    pl.semaphore_wait(barrier, len(places))


def gather_project(
    hid_ref,
    gain_ref,
    up_ref,
    base_ref,
    shift_ref,
    *rest,
):
    weights = rest[:7]
    q_ref, k_ref, vt_ref, r_ref, rk_ref, rv_ref, ld_ref = rest[7:14]
    hbuf, wbuf, acc, sumsq, wsem, ssem, rsem = rest[14:]
    y = lax.axis_index("y")
    c = lax.axis_index("c")
    other = 1 - c
    up, down, across = lax.rem(y + 1, NY), lax.rem(y + 3, NY), lax.rem(y + 2, NY)
    loads = []
    for n, w in enumerate(weights):
        load = pltpu.make_async_copy(w, wbuf.at[:, pl.ds(n * 128, 128)], wsem.at[n])
        load.start()
        loads.append(load)
    to_up, to_down, to_other = {"y": up}, {"y": down}, {"c": other}
    greet([to_up, to_down, to_other])

    own = y * 2 + c

    def send(n, src, dst, where):
        copy = remote(src, dst, ssem.at[n], rsem.at[n], where)
        copy.start()
        return copy

    first, second = pl.ds(0, HALF), pl.ds(HALF, HALF)
    copies = [None] * 9
    copies[0] = send(0, hid_ref, hbuf.at[own], to_up)
    copies[1] = send(1, hid_ref, hbuf.at[own], to_down)
    copies[2] = send(2, hid_ref, hbuf.at[own], to_other)
    for load in loads:
        load.wait()

    def add(block, number, fresh=False):
        w = wbuf[pl.ds(pl.multiple_of(number * FEAT, FEAT), FEAT), :]
        gain = gain_ref[pl.ds(number, 1), :]

        @pl.loop(0, ROWS // 128)
        def _(t):
            rows = pl.ds(pl.multiple_of(t * 128, 128), 128)
            h = block[rows, :].astype(F32)
            squares = h[:, :128] * h[:, :128] + h[:, 128:] * h[:, 128:]
            product = dot((h * gain).astype(BF16), w)
            if fresh:
                sumsq[rows, :] = squares
                acc[rows, :] = product
            else:
                sumsq[rows, :] += squares
                acc[rows, :] += product

    add(hid_ref, own, True)
    copies[2].wait_recv()
    add(hbuf.at[y * 2 + other], y * 2 + other)
    copies[0].wait_recv()
    below = hbuf.at[down * 2 + c]
    copies[3] = send(3, below.at[first], below.at[first], to_up)
    copies[4] = send(4, below, below, to_other)
    copies[1].wait_recv()
    above = hbuf.at[up * 2 + c]
    copies[5] = send(5, above.at[second], above.at[second], to_down)
    copies[6] = send(6, above, above, to_other)
    add(below, down * 2 + c)
    add(above, up * 2 + c)
    copies[4].wait_recv()
    add(hbuf.at[down * 2 + other], down * 2 + other)
    copies[6].wait_recv()
    add(hbuf.at[up * 2 + other], up * 2 + other)
    far = hbuf.at[across * 2 + c]
    copies[3].wait_recv()
    copies[7] = send(7, far.at[first], far.at[first], to_other)
    copies[5].wait_recv()
    copies[8] = send(8, far.at[second], far.at[second], to_other)
    add(far, across * 2 + c)
    copies[7].wait_recv()
    copies[8].wait_recv()
    add(hbuf.at[across * 2 + other], across * 2 + other)

    @pl.loop(0, ROWS // 128)
    def _(t):
        rows = pl.ds(pl.multiple_of(t * 128, 128), 128)
        total = jnp.sum(sumsq[rows, :], axis=1, keepdims=True)
        scale = lax.rsqrt(total * (1.0 / D) + NORM_EPS)
        r_ref[rows, :] = (acc[rows, 0:128] * scale).astype(BF16)
        rk_ref[rows, :] = (acc[rows, 128:256] * scale).astype(BF16)
        rv_ref[rows, :] = (acc[rows, 256:384] * scale).astype(BF16)
        low = jnp.tanh(acc[rows, 384:512] * scale).astype(BF16)
        gate = dot(low, up_ref[...]) + base_ref[...]
        ld_ref[rows, :] = -DECAY_SCALE * jax.nn.sigmoid(gate) + shift_ref[rows, :]
        q_ref[rows, :] = (acc[rows, 512:640] * (scale * (LOG2E * HD**-0.5))).astype(BF16)
        k_ref[rows, :] = (acc[rows, 640:768] * scale).astype(BF16)

    total = jnp.sum(sumsq[...], axis=1, keepdims=True)
    scale = lax.rsqrt(total * (1.0 / D) + NORM_EPS)
    vt_ref[...] = jnp.transpose(acc[:, 768:896] * scale).astype(BF16)
    for copy in copies:
        copy.wait_send()


def run_gather_project(hid, gain, up, base, shift, weights):
    whole = pl.BlockSpec(memory_space=VMEM)
    far = pl.BlockSpec(memory_space=pl.ANY)
    rows = jax.ShapeDtypeStruct((ROWS, 128), BF16)
    return pl.pallas_call(
        gather_project,
        out_shape=(
            rows,
            rows,
            jax.ShapeDtypeStruct((128, ROWS), BF16),
            rows,
            rows,
            rows,
            jax.ShapeDtypeStruct((ROWS, 128), F32),
        ),
        in_specs=[whole] * 5 + [far] * 7,
        out_specs=(whole,) * 7,
        scratch_shapes=[
            VMEM((NY * NC, ROWS, FEAT), BF16),
            VMEM((D, 896), BF16),
            VMEM((ROWS, 896), F32),
            VMEM((ROWS, 128), F32),
            pltpu.SemaphoreType.DMA((7,)),
            pltpu.SemaphoreType.DMA((9,)),
            pltpu.SemaphoreType.DMA((9,)),
        ],
        compiler_params=pltpu.CompilerParams(
            collective_id=0, has_side_effects=True, vmem_limit_bytes=40 * 2**20
        ),
        name="gather_project",
    )(hid, gain, up, base, shift, *weights)


def iota(shape, dim):
    return lax.broadcasted_iota(jnp.int32, shape, dim)


def by_head(x):
    first = lax.rem(iota(x.shape, 1), 128) < HD
    zero = jnp.zeros_like(x)
    return jnp.concatenate([jnp.where(first, x, zero), jnp.where(first, zero, x)], 0)


def same_head(shape):
    return (iota(shape, 0) < HD) == (lax.rem(iota(shape, 1), 128) < HD)


def inverse(lower):
    row, col = iota((CHUNK, CHUNK), 0), iota((CHUNK, CHUNK), 1)
    found = None
    size = 1
    while size < CHUNK:
        here = (
            (lax.div(row, 2 * size) == lax.div(col, 2 * size))
            & (lax.rem(row, 2 * size) >= size)
            & (lax.rem(col, 2 * size) < size)
        )
        part = jnp.where(here, lower, 0.0)
        if found is None:
            found = jnp.where(row == col, 1.0, part)
        else:
            found = found + coarse_dot(coarse_dot(found, part), found)
        size *= 2
    return found


def chunk_terms(r, k, v, w, rate):
    row, col = iota((CHUNK, CHUNK), 0), iota((CHUNK, CHUNK), 1)
    causal = (row >= col).astype(F32)
    running = jnp.dot(causal, w, precision=HIGHEST, preferred_element_type=F32)
    before = running - w
    ending = running[CHUNK - 1 :, :]
    first = col < HD
    square = k * k
    norm_one = jnp.sum(jnp.where(first, square, 0.0), axis=1, keepdims=True)
    norm_two = jnp.sum(jnp.where(first, 0.0, square), axis=1, keepdims=True)
    unit = k * jnp.where(first, lax.rsqrt(norm_one + KEY_EPS), lax.rsqrt(norm_two + KEY_EPS))
    erasing = unit * rate
    against = -unit
    pieces = []
    for i in range(CHUNK // SUB):
        at = slice(i * SUB, (i + 1) * SUB)
        start = running[i * SUB - 1 : i * SUB, :] if i else jnp.zeros_like(ending)
        left = jnp.concatenate(
            [
                against[at] * jnp.exp(before[at] - start),
                r[at] * jnp.exp(running[at] - start),
            ],
            0,
        )
        growth = jnp.exp(jnp.where(row < (i + 1) * SUB, start - running, -100.0))
        right = jnp.concatenate([erasing * growth, k * growth], 0)
        pieces.append(fine_dot_nt(by_head(left), right))

    def matrix(head, read, keys, keep):
        at = head * 2 * SUB + read * SUB
        whole = jnp.concatenate(
            [p[at : at + SUB, keys * CHUNK : (keys + 1) * CHUNK] for p in pieces], 0
        )
        return jnp.where(keep, whole, 0.0)

    strict, causal = row > col, row >= col
    inverses = [inverse(matrix(h, 0, 0, strict)) for h in range(2)]
    carry = [matrix(h, 0, 1, strict).astype(BF16) for h in range(2)]
    read_erase = [matrix(h, 1, 0, causal).astype(BF16) for h in range(2)]
    read_keys = [matrix(h, 1, 1, causal).astype(BF16) for h in range(2)]
    values = by_head(v)
    carried = dot(jnp.concatenate(carry, 1), values)
    right_side = by_head(jnp.concatenate([against * jnp.exp(before), carried], 1))
    solved = fine_dot(jnp.concatenate(inverses, 1), right_side)
    seen = dot(jnp.concatenate(read_erase, 1), by_head(solved.astype(BF16)))
    read_state = r * jnp.exp(running) + seen[:, :128]
    local = seen[:, 128:] + dot(jnp.concatenate(read_keys, 1), values)
    to_end = jnp.exp(ending - running)
    left = jnp.concatenate(
        [jnp.transpose(erasing * to_end), jnp.transpose(k * to_end)], 1
    )
    none = jnp.zeros((CHUNK, 128), F32)
    right = jnp.concatenate(
        [solved, jnp.concatenate([none, v.astype(F32)], 1)], 0
    )
    step = jnp.where(same_head((128, 256)), fine_dot(left, right), 0.0)
    wide_row, wide_col = iota((128, 256), 0), iota((128, 256), 1)
    decayed = jnp.concatenate([jnp.broadcast_to(jnp.exp(ending), (128, 128)), none], 1)
    step = step + jnp.where(wide_row == wide_col, decayed, 0.0)
    return read_state, local, step


def compose(later, earlier):
    out = fine_dot(later[:, :128], earlier)
    none = jnp.zeros((128, 128), F32)
    return out + jnp.concatenate([none, later[:, 128:]], 1)


def packed(step):
    return step[:HD] + step[HD:]


def unpacked(step):
    both = jnp.concatenate([step, step], 0)
    return jnp.where(same_head((128, 256)), both, 0.0)


def packed_identity():
    row, col = iota((HD, 256), 0), iota((HD, 256), 1)
    return jnp.where((col < 128) & (lax.rem(col, HD) == row), 1.0, 0.0)


def mixers(
    lam_ref,
    q_ref,
    k_ref,
    vt_ref,
    r_ref,
    rk_ref,
    rv_ref,
    ld_ref,
    rate_ref,
    mix_ref,
    sums_ref,
    kbuf,
    vbuf,
    qbuf,
    qwide,
    acc,
    top,
    low,
    osend,
    orecv,
    stsend,
    strecv,
    gxsend,
    gxbuf,
    gzsend,
    gzbuf,
    reads,
    local,
    ssem,
    rsem,
):
    z = lax.axis_index("z")
    x = lax.axis_index("x")
    z_up, z_down = {"z": lax.rem(z + 1, NZ)}, {"z": lax.rem(z + NZ - 1, NZ)}
    z_others = [{"z": lax.rem(z + n, NZ)} for n in range(1, NZ)]
    x_others = [lax.rem(x + n, NX) for n in range(1, NX)]
    greet(z_others + [{"x": n} for n in x_others])

    copies = []

    def send(src, dst, where):
        n = len(copies)
        copy = remote(src, dst, ssem.at[n], rsem.at[n], where)
        copy.start()
        copies.append(copy)
        return copy

    def forward(k_src, v_src, slot, where):
        return (
            send(k_src, kbuf.at[slot], where),
            send(v_src, vbuf.at[slot], where),
        )

    def arrived(pair):
        for copy in pair:
            copy.wait_recv()

    up1 = forward(k_ref, vt_ref, 0, z_up)
    down1 = forward(k_ref, vt_ref, 3, z_down)
    q_copies = [send(q_ref, qbuf.at[x], {"x": n}) for n in x_others]

    rate = rate_ref[...]
    so_far = None
    for n in range(ROWS // CHUNK):
        at = slice(n * CHUNK, (n + 1) * CHUNK)
        read_state, here, step = chunk_terms(
            r_ref[at, :].astype(F32),
            rk_ref[at, :].astype(F32),
            rv_ref[at, :],
            ld_ref[at, :],
            rate,
        )
        if so_far is None:
            reads[at, :] = read_state
            local[at, :] = here
            so_far = step
        else:
            seen = fine_dot(read_state, so_far)
            reads[at, :] = seen[:, :128]
            local[at, :] = here + seen[:, 128:]
            so_far = compose(step, so_far)
    gxsend[...] = packed(so_far)
    gxbuf[x] = packed(so_far)
    gx_copies = [send(gxsend, gxbuf.at[x], {"x": n}) for n in x_others]

    arrived(up1)
    up2 = forward(kbuf.at[0], vbuf.at[0], 1, z_up)
    arrived(down1)
    down2 = forward(kbuf.at[3], vbuf.at[3], 4, z_down)

    top[...] = jnp.full((NX, 8, 2 * ROWS), NEGATIVE, F32)
    low[...] = jnp.zeros((NX, 8, 2 * ROWS), F32)
    acc[...] = jnp.zeros((NX, 128, 2 * ROWS), F32)
    qbuf[x] = q_ref[...]
    for copy in q_copies:
        copy.wait_recv()
    for j in range(NX):
        qwide[j] = by_head(qbuf[j])

    def attend_one(k_block, v_block, j, masked):
        for t in range(3):
            cols = slice(t * 256, (t + 1) * 256)
            scores = dot_nt(k_block[...], qwide[j, cols, :])
            if masked:
                key_at = iota((ROWS, 256), 0)
                query_at = lax.rem(iota((ROWS, 256), 1) + t * 256, ROWS)
                scores = jnp.where(query_at >= key_at, scores, NEGATIVE)
            old = top[j, 0:1, cols]
            new = jnp.maximum(old, jnp.max(scores, axis=0, keepdims=True))
            weights = jnp.exp2(scores - new)
            rescale = jnp.exp2(old - new)
            top[j, 0:1, cols] = new
            low[j, 0:1, cols] = low[j, 0:1, cols] * rescale + jnp.sum(
                weights, axis=0, keepdims=True
            )
            acc[j, :, cols] = acc[j, :, cols] * rescale + dot(
                v_block[...], weights.astype(BF16)
            )

    def attend(slot, needed):
        @pl.when(needed)
        def _():
            @pl.loop(0, NX)
            def _(j):
                attend_one(kbuf.at[slot], vbuf.at[slot], j, False)

    attend_one(k_ref, vt_ref, x, True)

    @pl.loop(0, NX)
    def _(j):
        @pl.when(j > x)
        def _():
            attend_one(k_ref, vt_ref, j, False)

    attend(0, z >= 1)
    attend(3, z >= NZ - 1)

    for copy in gx_copies:
        copy.wait_recv()
    none = jnp.zeros((128, 128), F32)
    identity = jnp.where(iota((128, 256), 0) == iota((128, 256), 1), 1.0, 0.0)
    before_x = identity
    total = unpacked(gxbuf[0])
    for n in range(1, NX):
        before_x = jnp.where(x == n, total, before_x)
        total = compose(unpacked(gxbuf[n]), total)
    share = (packed(total) - packed_identity()).astype(BF16)
    gzsend[...] = share
    gzbuf[z] = share
    gz_copies = [send(gzsend, gzbuf.at[z], place) for place in z_others]

    arrived(up2)
    up3 = forward(kbuf.at[1], vbuf.at[1], 2, z_up)
    arrived(down2)
    down3 = forward(kbuf.at[4], vbuf.at[4], 5, z_down)
    attend(1, z >= 2)
    attend(4, z >= NZ - 2)

    arrived(up3)
    key_one, key_two = pl.ds(0, HALF), pl.ds(HALF, HALF)
    value_one, value_two = pl.ds(0, HD), pl.ds(HD, HD)
    up4 = (
        send(kbuf.at[2, key_one], kbuf.at[6, key_one], z_up),
        send(vbuf.at[2, value_one], vbuf.at[6, value_one], z_up),
    )
    arrived(down3)
    down4 = (
        send(kbuf.at[5, key_two], kbuf.at[6, key_two], z_down),
        send(vbuf.at[5, value_two], vbuf.at[6, value_two], z_down),
    )
    attend(2, z >= 3)
    attend(5, z >= NZ - 3)

    for copy in gz_copies:
        copy.wait_recv()
    state = none
    for n in range(NZ - 1):
        step = unpacked(gzbuf[n].astype(F32) + packed_identity())
        after = fine_dot(step[:, :128], state) + step[:, 128:]
        state = jnp.where(n < z, after, state)
    state = fine_dot(before_x[:, :128], state) + before_x[:, 128:]
    recurrent = local[...] + fine_dot(reads[...], state)
    first = iota((ROWS, 128), 1) < HD

    def head_mean(values):
        one = jnp.sum(jnp.where(first, values, 0.0), axis=1, keepdims=True)
        two = jnp.sum(jnp.where(first, 0.0, values), axis=1, keepdims=True)
        return jnp.where(first, one, two) * (1.0 / HD)

    centered = recurrent - head_mean(recurrent)
    normal = centered * lax.rsqrt(head_mean(centered * centered) + GROUP_EPS)
    mix_ref[:, 0:128] = normal.astype(BF16)

    arrived(up4)
    arrived(down4)
    attend(6, z >= 4)

    def partial_out(j):
        total = jnp.maximum(low[j, 0:1, :], TINY)
        return acc[j] * (1.0 / total), top[j, 0:1, :] + jnp.log2(total)

    o_copies = []
    for n in (1, 0, 2):
        j = x_others[n]
        out, level = partial_out(j)
        osend[n] = out.astype(BF16)
        stsend[n] = jnp.broadcast_to(level, (8, 2 * ROWS))
        o_copies.append(send(osend.at[n], orecv.at[n], {"x": j}))
        o_copies.append(send(stsend.at[n], strecv.at[n], {"x": j}))
    own_out, own_level = partial_out(x)
    for copy in o_copies:
        copy.wait_recv()
    levels = [own_level] + [strecv[n, 0:1, :] for n in range(3)]
    highest = functools.reduce(jnp.maximum, levels)
    shares = [jnp.exp2(level - highest) for level in levels]
    share_sum = sum(shares)
    map_out = own_out * (shares[0] / share_sum)
    for n in range(3):
        map_out = map_out + orecv[n].astype(F32) * (shares[n + 1] / share_sum)
    sums = (highest + jnp.log2(share_sum)) * LN2
    sums_ref[0:1, :] = sums[:, :ROWS]
    sums_ref[1:2, :] = sums[:, ROWS:]
    head_out = map_out[:, :ROWS] - lam_ref[0] * map_out[:, ROWS:]
    head_out = head_out * lax.rsqrt(
        jnp.mean(head_out * head_out, axis=0, keepdims=True) + HEAD_EPS
    )
    mix_ref[:, 128:256] = jnp.transpose(head_out).astype(BF16)
    for copy in copies:
        copy.wait_send()


def run_mixers(lam, q, k, vt, r, rk, rv, ld, rate):
    whole = pl.BlockSpec(memory_space=VMEM)
    count = 16 + 3 + 3 + 7 + 6
    return pl.pallas_call(
        mixers,
        out_shape=(
            jax.ShapeDtypeStruct((ROWS, 256), BF16),
            jax.ShapeDtypeStruct((2, ROWS), F32),
        ),
        in_specs=[pl.BlockSpec(memory_space=pltpu.SMEM)] + [whole] * 8,
        out_specs=(whole, whole),
        scratch_shapes=[
            VMEM((7, ROWS, 128), BF16),
            VMEM((7, 128, ROWS), BF16),
            VMEM((NX, ROWS, 128), BF16),
            VMEM((NX, 2 * ROWS, 128), BF16),
            VMEM((NX, 128, 2 * ROWS), F32),
            VMEM((NX, 8, 2 * ROWS), F32),
            VMEM((NX, 8, 2 * ROWS), F32),
            VMEM((3, 128, 2 * ROWS), BF16),
            VMEM((3, 128, 2 * ROWS), BF16),
            VMEM((3, 8, 2 * ROWS), F32),
            VMEM((3, 8, 2 * ROWS), F32),
            VMEM((HD, 256), F32),
            VMEM((NX, HD, 256), F32),
            VMEM((HD, 256), BF16),
            VMEM((NZ, HD, 256), BF16),
            VMEM((ROWS, 128), F32),
            VMEM((ROWS, 128), F32),
            pltpu.SemaphoreType.DMA((count,)),
            pltpu.SemaphoreType.DMA((count,)),
        ],
        compiler_params=pltpu.CompilerParams(
            collective_id=1, has_side_effects=True, vmem_limit_bytes=48 * 2**20
        ),
        name="mixers",
    )(lam, q, k, vt, r, rk, rv, ld, rate)


def project_sum(
    mix_ref,
    gain_ref,
    wr_ref,
    wa_ref,
    out_ref,
    wbuf,
    psend,
    precv,
    pair,
    hsend,
    hrecv,
    wsem,
    ssem,
    rsem,
):
    y = lax.axis_index("y")
    c = lax.axis_index("c")
    other = 1 - c
    up, down, across = lax.rem(y + 1, NY), lax.rem(y + 3, NY), lax.rem(y + 2, NY)
    loads = [
        pltpu.make_async_copy(wr_ref, wbuf.at[pl.ds(0, 128)], wsem.at[0]),
        pltpu.make_async_copy(wa_ref, wbuf.at[pl.ds(128, 128)], wsem.at[1]),
    ]
    for load in loads:
        load.start()
    to_up, to_down, to_other = {"y": up}, {"y": down}, {"c": other}
    greet([to_up, to_down, to_other])
    share = ROWS // (NY * NC)
    order = [across, up, down, y]

    def rows_for(core):
        return jnp.concatenate(
            [
                mix_ref[pl.ds(pl.multiple_of((n * 2 + core) * share, share), share), :]
                for n in order
            ],
            0,
        )

    for load in loads:
        load.wait()

    theirs = rows_for(other)
    ours = rows_for(c)
    for t in range(8):
        cols = slice(t * 256, (t + 1) * 256)
        psend[:, cols] = dot(theirs, wbuf[:, cols]).astype(BF16)
    copies = []

    def send(src, dst, where):
        n = len(copies)
        copy = remote(src, dst, ssem.at[n], rsem.at[n], where)
        copy.start()
        copies.append(copy)
        return copy

    pairs = [
        send(psend.at[pl.ds(n * share, share)], precv.at[pl.ds(n * share, share)], to_other)
        for n in range(4)
    ]
    for t in range(8):
        cols = slice(t * 256, (t + 1) * 256)
        pair[:, cols] = dot(ours, wbuf[:, cols])
    one, two = slice(0, D // 2), slice(D // 2, D)

    def summed(n, half):
        at = slice(n * share, (n + 1) * share)
        return pair[at, half] + precv[at, half].astype(F32)

    pairs[0].wait_recv()
    hsend[0] = summed(0, one).astype(BF16)
    relay_up = send(hsend.at[0], hrecv.at[0], to_up)
    hsend[1] = summed(0, two).astype(BF16)
    relay_down = send(hsend.at[1], hrecv.at[1], to_down)
    pairs[1].wait_recv()
    hsend[2] = summed(1, two).astype(BF16)
    plain_up = send(hsend.at[2], hrecv.at[2], to_up)
    pairs[2].wait_recv()
    hsend[3] = summed(2, one).astype(BF16)
    plain_down = send(hsend.at[3], hrecv.at[3], to_down)
    relay_up.wait_recv()
    hsend[4] = (summed(1, one) + hrecv[0].astype(F32)).astype(BF16)
    merged_up = send(hsend.at[4], hrecv.at[4], to_up)
    relay_down.wait_recv()
    hsend[5] = (summed(2, two) + hrecv[1].astype(F32)).astype(BF16)
    merged_down = send(hsend.at[5], hrecv.at[5], to_down)
    pairs[3].wait_recv()
    plain_up.wait_recv()
    plain_down.wait_recv()
    left = summed(3, one) + hrecv[3].astype(F32)
    right = summed(3, two) + hrecv[2].astype(F32)
    merged_up.wait_recv()
    merged_down.wait_recv()
    left = left + hrecv[4].astype(F32)
    right = right + hrecv[5].astype(F32)
    total = jnp.sum(left * left, axis=1, keepdims=True) + jnp.sum(
        right * right, axis=1, keepdims=True
    )
    scale = lax.rsqrt(total * (1.0 / D) + NORM_EPS)
    out_ref[:, one] = (left * scale * gain_ref[:, one]).astype(BF16)
    out_ref[:, two] = (right * scale * gain_ref[:, two]).astype(BF16)
    for copy in copies:
        copy.wait_send()


def run_project_sum(mix, gain, wr, wa):
    whole = pl.BlockSpec(memory_space=VMEM)
    far = pl.BlockSpec(memory_space=pl.ANY)
    share = ROWS // (NY * NC)
    return pl.pallas_call(
        project_sum,
        out_shape=jax.ShapeDtypeStruct((share, D), BF16),
        in_specs=[whole, whole, far, far],
        out_specs=whole,
        scratch_shapes=[
            VMEM((256, D), BF16),
            VMEM((4 * share, D), BF16),
            VMEM((4 * share, D), BF16),
            VMEM((4 * share, D), F32),
            VMEM((6, share, D // 2), BF16),
            VMEM((6, share, D // 2), BF16),
            pltpu.SemaphoreType.DMA((2,)),
            pltpu.SemaphoreType.DMA((10,)),
            pltpu.SemaphoreType.DMA((10,)),
        ],
        compiler_params=pltpu.CompilerParams(
            collective_id=2, has_side_effects=True, vmem_limit_bytes=40 * 2**20
        ),
        name="project_sum",
    )(mix, gain, wr, wa)


def per_device(
    hidden_in,
    in_gain,
    receptance_weight,
    key_weight,
    value_weight,
    decay_down,
    decay_up,
    decay_base,
    decay_shift,
    learn_rate,
    query_pair,
    key_pair,
    value_pair,
    mix_lambda,
    out_recurrent,
    out_attention,
    out_gain,
):
    q, k, vt, r, rk, rv, ld = run_gather_project(
        hidden_in,
        in_gain.reshape(NY * NC, FEAT),
        decay_up,
        decay_base.reshape(1, 128),
        decay_shift,
        (
            receptance_weight,
            key_weight,
            value_weight,
            decay_down,
            query_pair.reshape(D, 128),
            key_pair.reshape(D, 128),
            value_pair.reshape(D, 128),
        ),
    )
    mix, sums = run_mixers(
        mix_lambda, q, k, vt, r, rk, rv, ld, learn_rate.reshape(1, 128)
    )
    layer_out = run_project_sum(mix, out_gain.reshape(1, D), out_recurrent, out_attention)
    return layer_out, sums.reshape(1, 2, ROWS)


def solution(mesh):
    split_mesh = Mesh(mesh.devices.reshape(NZ, NX, NY, NC), ("z", "x", "y", "c"))
    sp, tp = ("z", "x"), ("y", "c")
    placed = (
        P(sp, tp),
        P(),
        P(None, tp),
        P(None, tp),
        P(None, tp),
        P(),
        P(None, tp),
        P(tp),
        P(sp, tp),
        P(tp),
        P(None, tp, None),
        P(None, tp, None),
        P(None, tp, None),
        P(tp),
        P(tp, None),
        P(tp, None),
        P(),
    )
    return jax.shard_map(
        per_device,
        mesh=split_mesh,
        in_specs=placed,
        out_specs=(P((*sp, *tp), None), P(tp, None, sp)),
        check_vma=False,
    )
```

time: 472 us -> 109 us (0.23)
  the two profiles are of different devices: /device:TPU:1 before, /device:TPU:227 now
where the time goes in v1:
time: 109 us
  Pallas kernels  95.5 us (88%)
  local copies, waits for them, and re-layouts  11.9 us (11%)
  between operations  1.38 us (1%)
    pallas_call x1, Pallas kernels, run_mixers(): pl.pallas_call(mixers, out_shape=(jax.ShapeDtypeStruct((ROWS, 256), BF16)...  66.2 us
    pallas_call x1, Pallas kernels, run_gather_project(): pl.pallas_call(gather_project, out_shape=(rows, rows, jax.ShapeDtypeStruc...  16.5 us
    pallas_call x1, Pallas kernels, run_project_sum(): pl.pallas_call(project_sum, out_shape=jax.ShapeDtypeStruct((share, D), BF...  12.9 us
    unnamed x34, local copies, waits for them, and re-layouts  11.9 us

profile of v1, /device:TPU:227, one launch (start us, length us, event | category | flops | bytes accessed | tf_op | source)
XLA Modules:
  0.0 108.7 jit_solution(1176877299231620536)
XLA Ops:
  0.6 0.0 copy-start.15
  1.3 0.0 copy-done.15
  1.3 0.0 copy-start.13
  1.3 0.6 copy-done.13
  2.0 0.0 copy-start
  2.0 1.0 copy-done
  3.0 0.0 copy-start.1
  3.0 1.0 copy-done.1
  4.1 0.0 copy-start.2
  4.1 1.0 copy-done.2
  5.1 0.0 copy-start.3
  5.1 1.0 copy-done.3
  6.2 0.0 copy-start.4
  6.2 1.0 copy-done.4
  7.2 0.0 copy-start.5
  7.2 1.0 copy-done.5
  8.2 0.0 copy-start.6
  8.2 1.0 copy-done.6
  9.3 0.0 copy-start.9
  9.3 0.9 copy-done.9
  10.2 0.0 copy-start.10
  10.2 0.9 copy-done.10
  11.1 0.0 copy-start.11
  11.1 0.8 copy-done.11
  11.9 0.0 copy-start.14
  11.9 0.0 copy-start.8
  11.9 16.5 %gather_project.1 = (bf16[384,128]{1,0:T(8,128)(2,1)S(1)}, bf16[384,128]{1,0:T(8,128)(2,1)S(1)}, bf16[128,384]{1,0:T(8,128)(2,1)S(1)}, bf16[384,128]{1,0:T(8,128...) custom-call(bf16[384,256]{1,0:T(8,128)(2,1)S(1)} %copy-done.9, ...), custom_call_target="tpu_custom_call" | custom-call | tf_op jit(solution)/shard_map/gather_project/pallas_call | solution.py:192
  28.4 0.0 copy-start.7
  28.4 0.0 copy-done.14
  28.4 0.0 copy-start.12
  28.4 66.2 %mixers.1 = (bf16[384,256]{1,0:T(8,128)(2,1)S(1)}, f32[2,384]{1,0:T(2,128)S(1)}) custom-call(f32[1]{0:T(128)S(6)} %copy.21.lam_ref, bf16[384,128]{1,0:T(8,128)(2,1)S(1)} %get-tuple-element.11.q_ref, bf16[384,128]{1,0:T(8,128)(2,1)S(1)} %get-tuple-element.12.k_ref, bf16[128,384]{1,0:T(8,128)(2,1)S(1)} %get-tuple-element.13.vt_ref, ...), custom_call_target="tpu_custom_call" | custom-call | tf_op jit(solution)/shard_map/mixers/pallas_call | solution.py:571
  94.6 0.0 copy-done.8
  94.6 0.0 copy-done.7
  94.6 0.0 copy-done.12
  94.6 12.9 %project_sum.1 = bf16[48,2048]{1,0:T(8,128)(2,1)S(1)} custom-call(bf16[384,256]{1,0:T(8,128)(2,1)S(1)} %get-tuple-element.18.mix_ref, f32[1,2048]{1,0:T(1,128)S(1)} %bitcast.10, bf16[128,2048]{1,0:T(8,128)(2,1)S(1)} %copy-done.7, bf16[128,2048]{1,0:T(8,128)(2,1)S(1)} %copy-done.8), custom_call_target="tpu_custom_call" | custom-call | tf_op jit(solution)/shard_map/project_sum/pallas_call | solution.py:717
  107.5 0.7 copy.22
  108.2 0.6 copy.23
  (1 shorter events, 0.0 us)
Async XLA Ops:
  0.6 0.7 copy-start.15
  1.3 0.7 copy-start.13
  2.0 1.0 copy-start
  3.0 1.0 copy-start.1
  4.1 1.0 copy-start.2
  5.1 1.0 copy-start.3
  6.2 1.0 copy-start.4
  7.2 1.0 copy-start.5
  8.2 1.0 copy-start.6
  9.3 0.9 copy-start.9
  10.2 0.9 copy-start.10
  11.1 0.8 copy-start.11
  11.9 16.5 %copy-start.14 = (f32[128]{0:T(128)S(1)}, f32[128]{0:T(128)}, u32[]{:S(2)}) copy-start(f32[128]{0:T(128)} %param.26) | copy-start | bytes 1540
  11.9 82.7 %copy-start.8 = (bf16[128,2048]{1,0:T(8,128)(2,1)S(1)}, bf16[128,2048]{1,0:T(8,128)(2,1)}, u32[]{:S(2)}) copy-start(bf16[128,2048]{1,0:T(8,128)(2,1)} %wa_ref.1) | copy-start | bytes 1572868
  28.4 66.2 %copy-start.7 = (bf16[128,2048]{1,0:T(8,128)(2,1)S(1)}, bf16[128,2048]{1,0:T(8,128)(2,1)}, u32[]{:S(2)}) copy-start(bf16[128,2048]{1,0:T(8,128)(2,1)} %wr_ref.1) | copy-start | bytes 1572868
  28.4 66.2 %copy-start.12 = (f32[2048]{0:T(1024)S(1)}, f32[2048]{0:T(1024)}, u32[]{:S(2)}) copy-start(f32[2048]{0:T(1024)} %param.33) | copy-start | bytes 24580

commit v2 on v1

v2 whole, which is shorter than its diff:
```python
import functools
import math

import jax
import jax.numpy as jnp
from jax import lax
from jax.experimental import pallas as pl
from jax.experimental.pallas import tpu as pltpu
from jax.sharding import Mesh
from jax.sharding import PartitionSpec as P

F32 = jnp.float32
BF16 = jnp.bfloat16
HD = 64
NZ, NX, NY, NC = 8, 4, 4, 2
ROWS = 384
HALF = ROWS // 2
D = 2048
FEAT = 256
CHUNK = 128
SUB = 32
DECAY_SCALE = math.exp(-0.5)
NORM_EPS = 1e-06
GROUP_EPS = 0.00064
HEAD_EPS = 1e-05
KEY_EPS = 1e-06
NEGATIVE = -1e30
TINY = 1e-37
LOG2E = 1.4426950408889634
LN2 = 0.6931471805599453
MESH = pl.DeviceIdType.MESH
VMEM = pltpu.VMEM
HIGHEST = lax.Precision.HIGHEST


def dot(a, b):
    return jnp.dot(a, b, preferred_element_type=F32)


def dot_nt(a, b):
    return lax.dot_general(a, b, (((1,), (1,)), ((), ())), preferred_element_type=F32)


def split(x):
    high = x.astype(BF16)
    return high, (x - high.astype(F32)).astype(BF16)


def fine_dot(a, b):
    a_high, a_low = split(a)
    b_high, b_low = split(b)
    both = dot(jnp.concatenate([a_high, a_low], 1), jnp.concatenate([b_high, b_high], 0))
    return both + dot(a_high, b_low)


def fine_dot_nt(a, b):
    a_high, a_low = split(a)
    b_high, b_low = split(b)
    both = dot_nt(jnp.concatenate([a_high, a_low], 1), jnp.concatenate([b_high, b_high], 1))
    return both + dot_nt(a_high, b_low)


def coarse_dot(a, b):
    return dot(a.astype(BF16), b.astype(BF16))


def remote(src, dst, send_sem, recv_sem, where):
    return pltpu.make_async_remote_copy(
        src_ref=src,
        dst_ref=dst,
        send_sem=send_sem,
        recv_sem=recv_sem,
        device_id=where,
        device_id_type=MESH,
    )


def greet(places):
    barrier = pltpu.get_barrier_semaphore()
    for place in places:
        pl.semaphore_signal(barrier, inc=1, device_id=place, device_id_type=MESH)
    pl.semaphore_wait(barrier, len(places))


def iota(shape, dim):
    return lax.broadcasted_iota(jnp.int32, shape, dim)


def by_head(x):
    first = lax.rem(iota(x.shape, 1), 128) < HD
    zero = jnp.zeros_like(x)
    return jnp.concatenate([jnp.where(first, x, zero), jnp.where(first, zero, x)], 0)


def same_head(shape):
    return (iota(shape, 0) < HD) == (lax.rem(iota(shape, 1), 128) < HD)


def inverse(lower):
    row, col = iota((CHUNK, CHUNK), 0), iota((CHUNK, CHUNK), 1)
    found = None
    size = 1
    while size < CHUNK:
        here = (
            (lax.div(row, 2 * size) == lax.div(col, 2 * size))
            & (lax.rem(row, 2 * size) >= size)
            & (lax.rem(col, 2 * size) < size)
        )
        part = jnp.where(here, lower, 0.0)
        if found is None:
            found = jnp.where(row == col, 1.0, part)
        else:
            found = found + coarse_dot(coarse_dot(found, part), found)
        size *= 2
    return found


def chunk_terms(r, k, v, w, rate):
    row, col = iota((CHUNK, CHUNK), 0), iota((CHUNK, CHUNK), 1)
    causal = (row >= col).astype(F32)
    running = jnp.dot(causal, w, precision=HIGHEST, preferred_element_type=F32)
    before = running - w
    ending = running[CHUNK - 1 :, :]
    first = col < HD
    square = k * k
    norm_one = jnp.sum(jnp.where(first, square, 0.0), axis=1, keepdims=True)
    norm_two = jnp.sum(jnp.where(first, 0.0, square), axis=1, keepdims=True)
    unit = k * jnp.where(first, lax.rsqrt(norm_one + KEY_EPS), lax.rsqrt(norm_two + KEY_EPS))
    erasing = unit * rate
    against = -unit
    pieces = []
    for i in range(CHUNK // SUB):
        at = slice(i * SUB, (i + 1) * SUB)
        start = running[i * SUB - 1 : i * SUB, :] if i else jnp.zeros_like(ending)
        left = jnp.concatenate(
            [
                against[at] * jnp.exp(before[at] - start),
                r[at] * jnp.exp(running[at] - start),
            ],
            0,
        )
        growth = jnp.exp(jnp.where(row < (i + 1) * SUB, start - running, -100.0))
        right = jnp.concatenate([erasing * growth, k * growth], 0)
        pieces.append(fine_dot_nt(by_head(left), right))

    def matrix(head, read, keys, keep):
        at = head * 2 * SUB + read * SUB
        whole = jnp.concatenate(
            [p[at : at + SUB, keys * CHUNK : (keys + 1) * CHUNK] for p in pieces], 0
        )
        return jnp.where(keep, whole, 0.0)

    strict, causal = row > col, row >= col
    inverses = [inverse(matrix(h, 0, 0, strict)) for h in range(2)]
    carry = [matrix(h, 0, 1, strict).astype(BF16) for h in range(2)]
    read_erase = [matrix(h, 1, 0, causal).astype(BF16) for h in range(2)]
    read_keys = [matrix(h, 1, 1, causal).astype(BF16) for h in range(2)]
    values = by_head(v)
    carried = dot(jnp.concatenate(carry, 1), values)
    right_side = by_head(jnp.concatenate([against * jnp.exp(before), carried], 1))
    solved = fine_dot(jnp.concatenate(inverses, 1), right_side)
    seen = dot(jnp.concatenate(read_erase, 1), by_head(solved.astype(BF16)))
    read_state = r * jnp.exp(running) + seen[:, :128]
    local = seen[:, 128:] + dot(jnp.concatenate(read_keys, 1), values)
    to_end = jnp.exp(ending - running)
    left = jnp.concatenate(
        [jnp.transpose(erasing * to_end), jnp.transpose(k * to_end)], 1
    )
    none = jnp.zeros((CHUNK, 128), F32)
    right = jnp.concatenate(
        [solved, jnp.concatenate([none, v.astype(F32)], 1)], 0
    )
    step = jnp.where(same_head((128, 256)), fine_dot(left, right), 0.0)
    wide_row, wide_col = iota((128, 256), 0), iota((128, 256), 1)
    decayed = jnp.concatenate([jnp.broadcast_to(jnp.exp(ending), (128, 128)), none], 1)
    step = step + jnp.where(wide_row == wide_col, decayed, 0.0)
    return read_state, local, step


def compose(later, earlier):
    out = fine_dot(later[:, :128], earlier)
    none = jnp.zeros((128, 128), F32)
    return out + jnp.concatenate([none, later[:, 128:]], 1)


def packed(step):
    return step[:HD] + step[HD:]


def unpacked(step):
    both = jnp.concatenate([step, step], 0)
    return jnp.where(same_head((128, 256)), both, 0.0)


def packed_identity():
    row, col = iota((HD, 256), 0), iota((HD, 256), 1)
    return jnp.where((col < 128) & (lax.rem(col, HD) == row), 1.0, 0.0)


class Courier:
    def __init__(self, ssem, rsem):
        self.ssem, self.rsem, self.copies = ssem, rsem, []

    def send(self, src, dst, where):
        n = len(self.copies)
        copy = remote(src, dst, self.ssem.at[n], self.rsem.at[n], where)
        copy.start()
        self.copies.append(copy)
        return copy


def load_all(places, sems, first):
    loads = []
    for n, (src, dst) in enumerate(places):
        load = pltpu.make_async_copy(src, dst, sems.at[first + n])
        load.start()
        loads.append(load)
    return loads


def layer(
    lam_ref,
    hid_hbm,
    gain_hbm,
    up_hbm,
    base_hbm,
    shift_hbm,
    rate_hbm,
    wr_hbm,
    wa_hbm,
    out_gain_hbm,
    *rest,
):
    weights = rest[:7]
    out_ref, sums_ref = rest[7:9]
    (
        hbuf,
        wbuf,
        proj,
        sumsq,
        gain_ref,
        up_ref,
        base_ref,
        shift_ref,
        rate_ref,
        out_w,
        out_gain_ref,
        q_ref,
        k_ref,
        vt_ref,
        r_ref,
        rk_ref,
        rv_ref,
        ld_ref,
        kbuf,
        vbuf,
        qbuf,
        qwide,
        acc,
        top,
        low,
        osend,
        orecv,
        stsend,
        strecv,
        gxsend,
        gxbuf,
        gzsend,
        gzbuf,
        reads,
        local,
        mix_ref,
        psend,
        precv,
        pair,
        hsend,
        hrecv,
        wsem,
        ssem,
        rsem,
    ) = rest[9:]
    z = lax.axis_index("z")
    x = lax.axis_index("x")
    y = lax.axis_index("y")
    c = lax.axis_index("c")
    other = 1 - c
    up, down, across = lax.rem(y + 1, NY), lax.rem(y + 3, NY), lax.rem(y + 2, NY)
    own = y * 2 + c
    loads = load_all([(hid_hbm, hbuf.at[own])], wsem, 0)
    places = [(w, wbuf.at[:, pl.ds(n * 128, 128)]) for n, w in enumerate(weights)]
    places += [
        (gain_hbm, gain_ref),
        (up_hbm, up_ref),
        (base_hbm, base_ref),
        (shift_hbm, shift_ref),
        (rate_hbm, rate_ref),
        (wr_hbm, out_w.at[pl.ds(0, 128)]),
        (wa_hbm, out_w.at[pl.ds(128, 128)]),
        (out_gain_hbm, out_gain_ref),
    ]
    loads += load_all(places, wsem, 1)
    to_up, to_down, to_other = {"y": up}, {"y": down}, {"c": other}
    z_up, z_down = {"z": lax.rem(z + 1, NZ)}, {"z": lax.rem(z + NZ - 1, NZ)}
    z_others = [{"z": lax.rem(z + n, NZ)} for n in range(1, NZ)]
    x_others = [lax.rem(x + n, NX) for n in range(1, NX)]
    greet([to_up, to_down, to_other, z_up, z_down] + [{"x": n} for n in x_others])
    courier = Courier(ssem, rsem)
    send = courier.send
    loads[0].wait()

    first, second = pl.ds(0, HALF), pl.ds(HALF, HALF)

    def share(number, part, where):
        block = hbuf.at[number]
        if part is not None:
            block = block.at[part]
        return send(block, block, where)

    below, above, far = down * 2 + c, up * 2 + c, across * 2 + c
    below_first = share(own, first, to_up)
    above_second = share(own, second, to_down)
    below_second = share(own, second, to_up)
    above_first = share(own, first, to_down)
    beside = share(own, None, to_other)
    for load in loads[1:]:
        load.wait()

    def add(number, fresh=False):
        block = hbuf.at[number]
        at = pl.multiple_of(number * FEAT, FEAT)
        w = wbuf[pl.ds(at, FEAT), :]
        gain = gain_ref[:, pl.ds(at, FEAT)]

        @pl.loop(0, ROWS // 128)
        def _(t):
            rows = pl.ds(pl.multiple_of(t * 128, 128), 128)
            h = block[rows, :].astype(F32)
            squares = h[:, :128] * h[:, :128] + h[:, 128:] * h[:, 128:]
            product = dot((h * gain).astype(BF16), w)
            if fresh:
                sumsq[rows, :] = squares
                proj[rows, :] = product
            else:
                sumsq[rows, :] += squares
                proj[rows, :] += product

    add(own, True)
    beside.wait_recv()
    add(y * 2 + other)
    below_first.wait_recv()
    far_first = share(below, first, to_up)
    relays = [share(below, first, to_other)]
    above_second.wait_recv()
    far_second = share(above, second, to_down)
    relays.append(share(above, second, to_other))
    below_second.wait_recv()
    relays.append(share(below, second, to_other))
    above_first.wait_recv()
    relays.append(share(above, first, to_other))
    add(below)
    add(above)
    far_first.wait_recv()
    relays.append(share(far, first, to_other))
    far_second.wait_recv()
    relays.append(share(far, second, to_other))
    relays[0].wait_recv()
    relays[2].wait_recv()
    add(down * 2 + other)
    relays[1].wait_recv()
    relays[3].wait_recv()
    add(up * 2 + other)
    add(far)
    relays[4].wait_recv()
    relays[5].wait_recv()
    add(across * 2 + other)

    total = jnp.sum(sumsq[...], axis=1, keepdims=True)
    scale = lax.rsqrt(total * (1.0 / D) + NORM_EPS)
    k_ref[...] = (proj[:, 640:768] * scale).astype(BF16)
    vt_ref[...] = jnp.transpose(proj[:, 768:896] * scale).astype(BF16)
    q_ref[...] = (proj[:, 512:640] * (scale * (LOG2E * HD**-0.5))).astype(BF16)

    def pass_on(buf, source, slot, first, second):
        source[0].wait_recv()
        ahead = send(buf.at[slot - 1, first], buf.at[slot if slot < 3 else 6, first], z_up)
        source[1].wait_recv()
        back = send(buf.at[slot + 2, second], buf.at[slot + 3, second], z_down)
        return ahead, back

    key_all, value_all = pl.ds(0, ROWS), pl.ds(0, 128)
    keys = (send(k_ref, kbuf.at[0], z_up), send(k_ref, kbuf.at[3], z_down))
    values = (send(vt_ref, vbuf.at[0], z_up), send(vt_ref, vbuf.at[3], z_down))
    q_copies = [send(q_ref, qbuf.at[x], {"x": x_others[n]}) for n in (1, 0, 2)]

    @pl.loop(0, ROWS // 128)
    def _(t):
        rows = pl.ds(pl.multiple_of(t * 128, 128), 128)
        total = jnp.sum(sumsq[rows, :], axis=1, keepdims=True)
        scale = lax.rsqrt(total * (1.0 / D) + NORM_EPS)
        r_ref[rows, :] = (proj[rows, 0:128] * scale).astype(BF16)
        rk_ref[rows, :] = (proj[rows, 128:256] * scale).astype(BF16)
        rv_ref[rows, :] = (proj[rows, 256:384] * scale).astype(BF16)
        down_low = jnp.tanh(proj[rows, 384:512] * scale).astype(BF16)
        gate = dot(down_low, up_ref[...]) + base_ref[...]
        ld_ref[rows, :] = -DECAY_SCALE * jax.nn.sigmoid(gate) + shift_ref[rows, :]

    rate = rate_ref[...]
    so_far = None
    for n in range(ROWS // CHUNK):
        at = slice(n * CHUNK, (n + 1) * CHUNK)
        read_state, here, step = chunk_terms(
            r_ref[at, :].astype(F32),
            rk_ref[at, :].astype(F32),
            rv_ref[at, :],
            ld_ref[at, :],
            rate,
        )
        if so_far is None:
            reads[at, :] = read_state
            local[at, :] = here
            so_far = step
        else:
            seen = fine_dot(read_state, so_far)
            reads[at, :] = seen[:, :128]
            local[at, :] = here + seen[:, 128:]
            so_far = compose(step, so_far)
    gxsend[...] = packed(so_far)
    gxbuf[x] = packed(so_far)
    gx_copies = [send(gxsend, gxbuf.at[x], {"x": n}) for n in x_others]

    keys = pass_on(kbuf, keys, 1, key_all, key_all)
    values = pass_on(vbuf, values, 1, value_all, value_all)

    qbuf[x] = q_ref[...]
    for copy in q_copies:
        copy.wait_recv()
    for j in range(NX):
        qwide[j] = by_head(qbuf[j])
    tiles = [slice(t * 256, (t + 1) * 256) for t in range(3)]

    def attend_all(k_block, v_block, own):
        k_all, v_all = k_block[...], v_block[...]

        def scores_of(j):
            found = [dot_nt(k_all, qwide[j, cols, :]) for cols in tiles]
            if own:
                for t in range(3):
                    key_at = iota((ROWS, 256), 0)
                    query_at = lax.rem(iota((ROWS, 256), 1) + t * 256, ROWS)
                    keep = query_at - key_at >= (x - j) * ROWS
                    found[t] = jnp.where(keep, found[t], NEGATIVE)
            return found, [jnp.max(s, axis=0, keepdims=True) for s in found]

        ready = scores_of(0)
        for j in range(NX):
            following = scores_of(j + 1) if j + 1 < NX else None
            scores, highest = ready
            if not own:
                olds = [top[j, 0:1, cols] for cols in tiles]
                sums = [low[j, 0:1, cols] for cols in tiles]
                totals = [acc[j, :, cols] for cols in tiles]
            for t, cols in enumerate(tiles):
                new = highest[t] if own else jnp.maximum(olds[t], highest[t])
                weights = jnp.exp2(scores[t] - new)
                part = jnp.sum(weights, axis=0, keepdims=True)
                seen = dot(v_all, weights.astype(BF16))
                top[j, 0:1, cols] = new
                if own:
                    low[j, 0:1, cols] = part
                    acc[j, :, cols] = seen
                else:
                    rescale = jnp.exp2(olds[t] - new)
                    low[j, 0:1, cols] = sums[t] * rescale + part
                    acc[j, :, cols] = totals[t] * rescale + seen
            ready = following

    def attend(slot, needed):
        @pl.when(needed)
        def _():
            attend_all(kbuf.at[slot], vbuf.at[slot], False)

    attend_all(k_ref, vt_ref, True)
    attend(0, z >= 1)
    keys = pass_on(kbuf, keys, 2, key_all, key_all)
    attend(3, z >= NZ - 1)
    values = pass_on(vbuf, values, 2, value_all, value_all)

    for copy in gx_copies:
        copy.wait_recv()
    none = jnp.zeros((128, 128), F32)
    identity = jnp.where(iota((128, 256), 0) == iota((128, 256), 1), 1.0, 0.0)
    before_x = identity
    total = unpacked(gxbuf[0])
    for n in range(1, NX):
        before_x = jnp.where(x == n, total, before_x)
        total = compose(unpacked(gxbuf[n]), total)
    share = (packed(total) - packed_identity()).astype(BF16)
    gzsend[...] = share
    gzbuf[z] = share

    attend(1, z >= 2)
    keys = pass_on(kbuf, keys, 3, pl.ds(0, HALF), pl.ds(HALF, HALF))
    attend(4, z >= NZ - 2)
    values = pass_on(vbuf, values, 3, pl.ds(0, HD), pl.ds(HD, HD))
    attend(2, z >= 3)
    attend(5, z >= NZ - 3)
    for copy in (*keys, *values):
        copy.wait_recv()
    gz_copies = [send(gzsend, gzbuf.at[z], place) for place in z_others]
    attend(6, z >= 4)

    def partial_out(j):
        total = jnp.maximum(low[j, 0:1, :], TINY)
        return acc[j] * (1.0 / total), top[j, 0:1, :] + jnp.log2(total)

    o_copies = []
    for n in (1, 0, 2):
        j = x_others[n]
        out, level = partial_out(j)
        osend[n] = out.astype(BF16)
        stsend[n] = jnp.broadcast_to(level, (8, 2 * ROWS))
        o_copies.append(send(osend.at[n], orecv.at[n], {"x": j}))
        o_copies.append(send(stsend.at[n], strecv.at[n], {"x": j}))
    own_out, own_level = partial_out(x)

    for copy in gz_copies:
        copy.wait_recv()
    state = none
    for n in range(NZ - 1):
        step = unpacked(gzbuf[n].astype(F32) + packed_identity())
        after = fine_dot(step[:, :128], state) + step[:, 128:]
        state = jnp.where(n < z, after, state)
    state = fine_dot(before_x[:, :128], state) + before_x[:, 128:]
    recurrent = local[...] + fine_dot(reads[...], state)
    first = iota((ROWS, 128), 1) < HD

    def head_mean(values):
        one = jnp.sum(jnp.where(first, values, 0.0), axis=1, keepdims=True)
        two = jnp.sum(jnp.where(first, 0.0, values), axis=1, keepdims=True)
        return jnp.where(first, one, two) * (1.0 / HD)

    centered = recurrent - head_mean(recurrent)
    normal = centered * lax.rsqrt(head_mean(centered * centered) + GROUP_EPS)
    mix_ref[:, 0:128] = normal.astype(BF16)

    for copy in o_copies:
        copy.wait_recv()
    levels = [own_level] + [strecv[n, 0:1, :] for n in range(3)]
    highest = functools.reduce(jnp.maximum, levels)
    shares = [jnp.exp2(level - highest) for level in levels]
    share_sum = sum(shares)
    map_out = own_out * (shares[0] / share_sum)
    for n in range(3):
        map_out = map_out + orecv[n].astype(F32) * (shares[n + 1] / share_sum)
    sums = (highest + jnp.log2(share_sum)) * LN2
    sums_ref[0:1, :] = sums[:, :ROWS]
    sums_ref[1:2, :] = sums[:, ROWS:]
    head_out = map_out[:, :ROWS] - lam_ref[0] * map_out[:, ROWS:]
    head_out = head_out * lax.rsqrt(
        jnp.mean(head_out * head_out, axis=0, keepdims=True) + HEAD_EPS
    )
    mix_ref[:, 128:256] = jnp.transpose(head_out).astype(BF16)

    part_rows = ROWS // (NY * NC)
    order = [across, up, down, y]

    def rows_for(core):
        return jnp.concatenate(
            [
                mix_ref[pl.ds(pl.multiple_of((n * 2 + core) * part_rows, part_rows), part_rows), :]
                for n in order
            ],
            0,
        )

    theirs = rows_for(other)
    ours = rows_for(c)
    for t in range(8):
        cols = slice(t * 256, (t + 1) * 256)
        psend[:, cols] = dot(theirs, out_w[:, cols]).astype(BF16)
    pairs = [
        send(psend.at[pl.ds(n * part_rows, part_rows)], precv.at[pl.ds(n * part_rows, part_rows)], to_other)
        for n in range(4)
    ]
    for t in range(8):
        cols = slice(t * 256, (t + 1) * 256)
        pair[:, cols] = dot(ours, out_w[:, cols])
    one, two = slice(0, D // 2), slice(D // 2, D)

    def summed(n, half):
        at = slice(n * part_rows, (n + 1) * part_rows)
        return pair[at, half] + precv[at, half].astype(F32)

    pairs[0].wait_recv()
    hsend[0] = summed(0, one).astype(BF16)
    relay_up = send(hsend.at[0], hrecv.at[0], to_up)
    hsend[1] = summed(0, two).astype(BF16)
    relay_down = send(hsend.at[1], hrecv.at[1], to_down)
    pairs[1].wait_recv()
    hsend[2] = summed(1, two).astype(BF16)
    plain_up = send(hsend.at[2], hrecv.at[2], to_up)
    pairs[2].wait_recv()
    hsend[3] = summed(2, one).astype(BF16)
    plain_down = send(hsend.at[3], hrecv.at[3], to_down)
    relay_up.wait_recv()
    hsend[4] = (summed(1, one) + hrecv[0].astype(F32)).astype(BF16)
    merged_up = send(hsend.at[4], hrecv.at[4], to_up)
    relay_down.wait_recv()
    hsend[5] = (summed(2, two) + hrecv[1].astype(F32)).astype(BF16)
    merged_down = send(hsend.at[5], hrecv.at[5], to_down)
    pairs[3].wait_recv()
    plain_up.wait_recv()
    plain_down.wait_recv()
    left_half = summed(3, one) + hrecv[3].astype(F32)
    right_half = summed(3, two) + hrecv[2].astype(F32)
    merged_up.wait_recv()
    merged_down.wait_recv()
    left_half = left_half + hrecv[4].astype(F32)
    right_half = right_half + hrecv[5].astype(F32)
    total = jnp.sum(left_half * left_half, axis=1, keepdims=True) + jnp.sum(
        right_half * right_half, axis=1, keepdims=True
    )
    scale = lax.rsqrt(total * (1.0 / D) + NORM_EPS)
    out_ref[:, one] = (left_half * scale * out_gain_ref[:, one]).astype(BF16)
    out_ref[:, two] = (right_half * scale * out_gain_ref[:, two]).astype(BF16)
    for copy in courier.copies:
        copy.wait_send()


def run_layer(lam, hid, gain, up, base, shift, rate, wr, wa, out_gain, weights):
    whole = pl.BlockSpec(memory_space=VMEM)
    far = pl.BlockSpec(memory_space=pl.ANY)
    share = ROWS // (NY * NC)
    count = 13 + 16 + 3 + 3 + 7 + 6 + 10
    rows = VMEM((ROWS, 128), BF16)
    return pl.pallas_call(
        layer,
        out_shape=(
            jax.ShapeDtypeStruct((share, D), BF16),
            jax.ShapeDtypeStruct((2, ROWS), F32),
        ),
        in_specs=[pl.BlockSpec(memory_space=pltpu.SMEM)] + [far] * 16,
        out_specs=(whole, whole),
        scratch_shapes=[
            VMEM((NY * NC, ROWS, FEAT), BF16),
            VMEM((D, 896), BF16),
            VMEM((ROWS, 896), F32),
            VMEM((ROWS, 128), F32),
            VMEM((1, D), F32),
            VMEM((128, 128), BF16),
            VMEM((1, 128), F32),
            VMEM((ROWS, 128), F32),
            VMEM((1, 128), F32),
            VMEM((256, D), BF16),
            VMEM((1, D), F32),
            rows,
            rows,
            VMEM((128, ROWS), BF16),
            rows,
            rows,
            rows,
            VMEM((ROWS, 128), F32),
            VMEM((7, ROWS, 128), BF16),
            VMEM((7, 128, ROWS), BF16),
            VMEM((NX, ROWS, 128), BF16),
            VMEM((NX, 2 * ROWS, 128), BF16),
            VMEM((NX, 128, 2 * ROWS), F32),
            VMEM((NX, 8, 2 * ROWS), F32),
            VMEM((NX, 8, 2 * ROWS), F32),
            VMEM((3, 128, 2 * ROWS), BF16),
            VMEM((3, 128, 2 * ROWS), BF16),
            VMEM((3, 8, 2 * ROWS), F32),
            VMEM((3, 8, 2 * ROWS), F32),
            VMEM((HD, 256), F32),
            VMEM((NX, HD, 256), F32),
            VMEM((HD, 256), BF16),
            VMEM((NZ, HD, 256), BF16),
            VMEM((ROWS, 128), F32),
            VMEM((ROWS, 128), F32),
            VMEM((ROWS, 256), BF16),
            VMEM((4 * share, D), BF16),
            VMEM((4 * share, D), BF16),
            VMEM((4 * share, D), F32),
            VMEM((6, share, D // 2), BF16),
            VMEM((6, share, D // 2), BF16),
            pltpu.SemaphoreType.DMA((16,)),
            pltpu.SemaphoreType.DMA((count,)),
            pltpu.SemaphoreType.DMA((count,)),
        ],
        compiler_params=pltpu.CompilerParams(
            collective_id=0, has_side_effects=True, vmem_limit_bytes=63 * 2**20
        ),
        name="layer",
    )(lam, hid, gain, up, base, shift, rate, wr, wa, out_gain, *weights)


def per_device(
    hidden_in,
    in_gain,
    receptance_weight,
    key_weight,
    value_weight,
    decay_down,
    decay_up,
    decay_base,
    decay_shift,
    learn_rate,
    query_pair,
    key_pair,
    value_pair,
    mix_lambda,
    out_recurrent,
    out_attention,
    out_gain,
):
    layer_out, sums = run_layer(
        mix_lambda,
        hidden_in,
        in_gain.reshape(1, D),
        decay_up,
        decay_base.reshape(1, 128),
        decay_shift,
        learn_rate.reshape(1, 128),
        out_recurrent,
        out_attention,
        out_gain.reshape(1, D),
        (
            receptance_weight,
            key_weight,
            value_weight,
            decay_down,
            query_pair.reshape(D, 128),
            key_pair.reshape(D, 128),
            value_pair.reshape(D, 128),
        ),
    )
    return layer_out, sums.reshape(1, 2, ROWS)


def solution(mesh):
    split_mesh = Mesh(mesh.devices.reshape(NZ, NX, NY, NC), ("z", "x", "y", "c"))
    sp, tp = ("z", "x"), ("y", "c")
    placed = (
        P(sp, tp),
        P(),
        P(None, tp),
        P(None, tp),
        P(None, tp),
        P(),
        P(None, tp),
        P(tp),
        P(sp, tp),
        P(tp),
        P(None, tp, None),
        P(None, tp, None),
        P(None, tp, None),
        P(tp),
        P(tp, None),
        P(tp, None),
        P(),
    )
    return jax.shard_map(
        per_device,
        mesh=split_mesh,
        in_specs=placed,
        out_specs=(P((*sp, *tp), None), P(tp, None, sp)),
        check_vma=False,
    )
```

time: 109 us -> 74 us (0.68)
  the two profiles are of different devices: /device:TPU:227 before, /device:TPU:1 now
where the time goes in v2:
time: 74 us; the launch traced here: 73.9 us
  Pallas kernels  70.4 us (95%)
  local copies, waits for them, and re-layouts  2.2 us (3%)
  between operations  1.3 us (2%)
    pallas_call x1, Pallas kernels, run_layer(): pl.pallas_call(layer, out_shape=(jax.ShapeDtypeStruct((share, D), BF16),...  70.4 us
    unnamed x4, local copies, waits for them, and re-layouts  2.2 us

profile of v2, /device:TPU:1, one launch (start us, length us, event | category | flops | bytes accessed | tf_op | source)
XLA Modules:
  0.0 73.9 jit_solution(14201514165466817357)
XLA Ops:
  1.3 70.4 %layer.1 = (bf16[48,2048]{1,0:T(8,128)(2,1)}, f32[2,384]{1,0:T(2,128)}) custom-call(f32[1]{0:T(128)S(6)} %copy.21.lam_ref, bf16[384,256]{1,0:T(8,128)(2,1)} %hid_hbm.1, f32[1,2048]{1,0:T(1,128)} %bitcast.11, bf16[128,128]{1,0:T(8,128)(2,1)} %up_hbm.1, f32[1,128]{1,0:T(1,128)} %bitcast.14, f32[384,128]{1,0:T(8,128)} %shift_hbm.1, f32[1,128]{1,0:T(1,128)} %bitcast.15, ...), custom_call_target="tpu_custom_call" | custom-call | tf_op jit(solution)/shard_map/layer/pallas_call | solution.py:636
  71.7 0.0 copy-start
  71.7 1.6 %copy.22 = bf16[48,2048]{1,0:T(8,128)(2,1)} copy(bf16[48,2048]{1,0:T(8,128)(2,1)} %get-tuple-element.8) | data formatting | bytes 393216
  73.3 0.0 copy-done
  73.3 0.6 copy.23
Async XLA Ops:
  71.7 1.6 %copy-start = (f32[2,384]{1,0:T(2,128)S(1)}, f32[2,384]{1,0:T(2,128)}, u32[]{:S(2)}) copy-start(f32[2,384]{1,0:T(2,128)} %get-tuple-element.5) | copy-start | bytes 9220

commit v3 on v2

--- a/solution.py
+++ b/solution.py
@@ -96,85 +96,137 @@
     return (iota(shape, 0) < HD) == (lax.rem(iota(shape, 1), 128) < HD)
 
 
-def inverse(lower):
+SIZES = ((1, 8), (8, 32), (32, 128))
+
+
+def blocks_mask(small, large):
     row, col = iota((CHUNK, CHUNK), 0), iota((CHUNK, CHUNK), 1)
+    return (lax.div(row, large) == lax.div(col, large)) & (lax.div(row, small) > lax.div(col, small))
+
+
+def inverses(lowers):
+    row, col = iota((CHUNK, CHUNK), 0), iota((CHUNK, CHUNK), 1)
+    identity = jnp.where(row == col, 1.0, 0.0)
     found = None
-    size = 1
-    while size < CHUNK:
-        here = (
-            (lax.div(row, 2 * size) == lax.div(col, 2 * size))
-            & (lax.rem(row, 2 * size) >= size)
-            & (lax.rem(col, 2 * size) < size)
+    for small, large in SIZES:
+        keep = blocks_mask(small, large)
+        parts = [jnp.where(keep, lower, 0.0) for lower in lowers]
+        if found is None:
+            steps = parts
+            found = [identity + part for part in parts]
+        else:
+            steps = [coarse_dot(f, part) for f, part in zip(found, parts)]
+            found = [f + coarse_dot(s, f) for f, s in zip(found, steps)]
+        reach = 2
+        while reach * small < large:
+            steps = [coarse_dot(s, s) for s in steps]
+            found = [f + coarse_dot(s, f) for f, s in zip(found, steps)]
+            reach *= 2
+    return found
+
+
+def all_terms(receptance, keys, values, decays, rate):
+    count = ROWS // CHUNK
+    cuts = [slice(n * CHUNK, (n + 1) * CHUNK) for n in range(count)]
+    row, col = iota((CHUNK, CHUNK), 0), iota((CHUNK, CHUNK), 1)
+    ones = (row >= col).astype(BF16)
+    first = col < HD
+    w = [decays[at, :] for at in cuts]
+    r = [receptance[at, :].astype(F32) for at in cuts]
+    k = [keys[at, :].astype(F32) for at in cuts]
+    v = [values[at, :] for at in cuts]
+    running = []
+    for part in w:
+        high = part.astype(BF16)
+        rest = part - high.astype(F32)
+        middle = rest.astype(BF16)
+        lowest = (rest - middle.astype(F32)).astype(BF16)
+        running.append(
+            dot(jnp.concatenate([ones, ones], 1), jnp.concatenate([high, middle], 0))
+            + dot(ones, lowest)
         )
-        part = jnp.where(here, lower, 0.0)
-        if found is None:
-            found = jnp.where(row == col, 1.0, part)
-        else:
-            found = found + coarse_dot(coarse_dot(found, part), found)
-        size *= 2
-    return found
-
-
-def chunk_terms(r, k, v, w, rate):
-    row, col = iota((CHUNK, CHUNK), 0), iota((CHUNK, CHUNK), 1)
-    causal = (row >= col).astype(F32)
-    running = jnp.dot(causal, w, precision=HIGHEST, preferred_element_type=F32)
-    before = running - w
-    ending = running[CHUNK - 1 :, :]
-    first = col < HD
-    square = k * k
-    norm_one = jnp.sum(jnp.where(first, square, 0.0), axis=1, keepdims=True)
-    norm_two = jnp.sum(jnp.where(first, 0.0, square), axis=1, keepdims=True)
-    unit = k * jnp.where(first, lax.rsqrt(norm_one + KEY_EPS), lax.rsqrt(norm_two + KEY_EPS))
-    erasing = unit * rate
-    against = -unit
-    pieces = []
+    before = [a - b for a, b in zip(running, w)]
+    ending = [a[CHUNK - 1 :, :] for a in running]
+    unit = []
+    for part in k:
+        square = part * part
+        one = jnp.sum(jnp.where(first, square, 0.0), axis=1, keepdims=True)
+        two = jnp.sum(jnp.where(first, 0.0, square), axis=1, keepdims=True)
+        unit.append(part * lax.rsqrt(jnp.where(first, one, two) + KEY_EPS))
+    erasing = [u * rate for u in unit]
+    pieces = [[] for _ in cuts]
     for i in range(CHUNK // SUB):
         at = slice(i * SUB, (i + 1) * SUB)
-        start = running[i * SUB - 1 : i * SUB, :] if i else jnp.zeros_like(ending)
-        left = jnp.concatenate(
-            [
-                against[at] * jnp.exp(before[at] - start),
-                r[at] * jnp.exp(running[at] - start),
-            ],
-            0,
-        )
-        growth = jnp.exp(jnp.where(row < (i + 1) * SUB, start - running, -100.0))
-        right = jnp.concatenate([erasing * growth, k * growth], 0)
-        pieces.append(fine_dot_nt(by_head(left), right))
-
-    def matrix(head, read, keys, keep):
+        for n in range(count):
+            start = running[n][i * SUB - 1 : i * SUB, :] if i else jnp.zeros_like(ending[n])
+            left = jnp.concatenate(
+                [
+                    -unit[n][at] * jnp.exp(before[n][at] - start),
+                    r[n][at] * jnp.exp(running[n][at] - start),
+                ],
+                0,
+            )
+            growth = jnp.exp(jnp.where(row < (i + 1) * SUB, start - running[n], -100.0))
+            right = jnp.concatenate([erasing[n] * growth, k[n] * growth], 0)
+            pieces[n].append(fine_dot_nt(by_head(left), right))
+
+    def matrix(n, head, read, which, keep):
         at = head * 2 * SUB + read * SUB
         whole = jnp.concatenate(
-            [p[at : at + SUB, keys * CHUNK : (keys + 1) * CHUNK] for p in pieces], 0
+            [p[at : at + SUB, which * CHUNK : (which + 1) * CHUNK] for p in pieces[n]], 0
         )
         return jnp.where(keep, whole, 0.0)
 
     strict, causal = row > col, row >= col
-    inverses = [inverse(matrix(h, 0, 0, strict)) for h in range(2)]
-    carry = [matrix(h, 0, 1, strict).astype(BF16) for h in range(2)]
-    read_erase = [matrix(h, 1, 0, causal).astype(BF16) for h in range(2)]
-    read_keys = [matrix(h, 1, 1, causal).astype(BF16) for h in range(2)]
-    values = by_head(v)
-    carried = dot(jnp.concatenate(carry, 1), values)
-    right_side = by_head(jnp.concatenate([against * jnp.exp(before), carried], 1))
-    solved = fine_dot(jnp.concatenate(inverses, 1), right_side)
-    seen = dot(jnp.concatenate(read_erase, 1), by_head(solved.astype(BF16)))
-    read_state = r * jnp.exp(running) + seen[:, :128]
-    local = seen[:, 128:] + dot(jnp.concatenate(read_keys, 1), values)
-    to_end = jnp.exp(ending - running)
-    left = jnp.concatenate(
-        [jnp.transpose(erasing * to_end), jnp.transpose(k * to_end)], 1
-    )
+    found = inverses([matrix(n, h, 0, 0, strict) for n in range(count) for h in range(2)])
+    found = [jnp.concatenate(found[2 * n : 2 * n + 2], 1) for n in range(count)]
+
+    def pair(n, read, which, keep):
+        return jnp.concatenate(
+            [matrix(n, h, read, which, keep).astype(BF16) for h in range(2)], 1
+        )
+
+    by_value = [by_head(part) for part in v]
+    carried = [dot(pair(n, 0, 1, strict), by_value[n]) for n in range(count)]
+    right_side = [
+        by_head(jnp.concatenate([-unit[n] * jnp.exp(before[n]), carried[n]], 1))
+        for n in range(count)
+    ]
+    solved = [fine_dot(found[n], right_side[n]) for n in range(count)]
+    seen = [
+        dot(pair(n, 1, 0, causal), by_head(solved[n].astype(BF16))) for n in range(count)
+    ]
+    local = [seen[n][:, 128:] + dot(pair(n, 1, 1, causal), by_value[n]) for n in range(count)]
+    read_state = [r[n] * jnp.exp(running[n]) + seen[n][:, :128] for n in range(count)]
     none = jnp.zeros((CHUNK, 128), F32)
-    right = jnp.concatenate(
-        [solved, jnp.concatenate([none, v.astype(F32)], 1)], 0
-    )
-    step = jnp.where(same_head((128, 256)), fine_dot(left, right), 0.0)
     wide_row, wide_col = iota((128, 256), 0), iota((128, 256), 1)
-    decayed = jnp.concatenate([jnp.broadcast_to(jnp.exp(ending), (128, 128)), none], 1)
-    step = step + jnp.where(wide_row == wide_col, decayed, 0.0)
-    return read_state, local, step
+    steps = []
+    for n in range(count):
+        to_end = jnp.exp(ending[n] - running[n])
+        left = jnp.concatenate(
+            [jnp.transpose(erasing[n] * to_end), jnp.transpose(k[n] * to_end)], 1
+        )
+        right = jnp.concatenate(
+            [solved[n], jnp.concatenate([none, v[n].astype(F32)], 1)], 0
+        )
+        step = jnp.where(same_head((128, 256)), fine_dot(left, right), 0.0)
+        decayed = jnp.concatenate(
+            [jnp.broadcast_to(jnp.exp(ending[n]), (128, 128)), none], 1
+        )
+        steps.append(step + jnp.where(wide_row == wide_col, decayed, 0.0))
+    return read_state, local, steps
+
+
+def device_terms(receptance, keys, values, decays, rate):
+    read_state, local, steps = all_terms(receptance, keys, values, decays, rate)
+    reads, reach = [read_state[0]], [local[0]]
+    so_far = steps[0]
+    for n in range(1, len(steps)):
+        seen = fine_dot(read_state[n], so_far)
+        reads.append(seen[:, :128])
+        reach.append(local[n] + seen[:, 128:])
+        so_far = compose(steps[n], so_far)
+    return reads, reach, so_far
 
 
 def compose(later, earlier):
@@ -404,26 +456,10 @@
         gate = dot(down_low, up_ref[...]) + base_ref[...]
         ld_ref[rows, :] = -DECAY_SCALE * jax.nn.sigmoid(gate) + shift_ref[rows, :]
 
-    rate = rate_ref[...]
-    so_far = None
+    found_reads, found_local, so_far = device_terms(r_ref, rk_ref, rv_ref, ld_ref, rate_ref[...])
     for n in range(ROWS // CHUNK):
-        at = slice(n * CHUNK, (n + 1) * CHUNK)
-        read_state, here, step = chunk_terms(
-            r_ref[at, :].astype(F32),
-            rk_ref[at, :].astype(F32),
-            rv_ref[at, :],
-            ld_ref[at, :],
-            rate,
-        )
-        if so_far is None:
-            reads[at, :] = read_state
-            local[at, :] = here
-            so_far = step
-        else:
-            seen = fine_dot(read_state, so_far)
-            reads[at, :] = seen[:, :128]
-            local[at, :] = here + seen[:, 128:]
-            so_far = compose(step, so_far)
+        reads[n * CHUNK : (n + 1) * CHUNK, :] = found_reads[n]
+        local[n * CHUNK : (n + 1) * CHUNK, :] = found_local[n]
     gxsend[...] = packed(so_far)
     gxbuf[x] = packed(so_far)
     gx_copies = [send(gxsend, gxbuf.at[x], {"x": n}) for n in x_others]
@@ -553,8 +589,8 @@
     for n in range(3):
         map_out = map_out + orecv[n].astype(F32) * (shares[n + 1] / share_sum)
     sums = (highest + jnp.log2(share_sum)) * LN2
-    sums_ref[0:1, :] = sums[:, :ROWS]
-    sums_ref[1:2, :] = sums[:, ROWS:]
+    sums_ref[0, 0:1, :] = sums[:, :ROWS]
+    sums_ref[0, 1:2, :] = sums[:, ROWS:]
     head_out = map_out[:, :ROWS] - lam_ref[0] * map_out[:, ROWS:]
     head_out = head_out * lax.rsqrt(
         jnp.mean(head_out * head_out, axis=0, keepdims=True) + HEAD_EPS
@@ -637,7 +673,7 @@
         layer,
         out_shape=(
             jax.ShapeDtypeStruct((share, D), BF16),
-            jax.ShapeDtypeStruct((2, ROWS), F32),
+            jax.ShapeDtypeStruct((1, 2, ROWS), F32),
         ),
         in_specs=[pl.BlockSpec(memory_space=pltpu.SMEM)] + [far] * 16,
         out_specs=(whole, whole),
@@ -734,7 +770,7 @@
             value_pair.reshape(D, 128),
         ),
     )
-    return layer_out, sums.reshape(1, 2, ROWS)
+    return layer_out, sums
 
 
 def solution(mesh):

time: 74 us -> 67.3 us (0.909)
  Pallas kernels: 70.4 us -> 63.7 us
    pallas_call x1, Pallas kernels: 70.4 us -> 63.7 us  [run_layer(): pl.pallas_call(layer, out_shape=(jax.ShapeDtypeStruct((share, D), BF16),...]
where the time goes in v3:
time: 67.3 us; the launch traced here: 67.2 us
  Pallas kernels  63.7 us (95%)
  local copies, waits for them, and re-layouts  2.2 us (3%)
  between operations  1.3 us (2%)
    pallas_call x1, Pallas kernels, run_layer(): pl.pallas_call(layer, out_shape=(jax.ShapeDtypeStruct((share, D), BF16),...  63.7 us
    unnamed x4, local copies, waits for them, and re-layouts  2.2 us

profile of v3, /device:TPU:1, one launch (start us, length us, event | category | flops | bytes accessed | tf_op | source)
XLA Modules:
  0.0 67.2 jit_solution(11565654529918433499)
XLA Ops:
  1.3 63.7 %layer.1 = (bf16[48,2048]{1,0:T(8,128)(2,1)}, f32[1,2,384]{2,1,0:T(2,128)}) custom-call(f32[1]{0:T(128)S(6)} %copy.21.lam_ref, bf16[384,256]{1,0:T(8,128)(2,1)} %hid_hbm.1, f32[1,2048]{1,0:T(1,128)} %bitcast.10, bf16[128,128]{1,0:T(8,128)(2,1)} %up_hbm.1, f32[1,128]{1,0:T(1,128)} %bitcast.12, f32[384,128]{1,0:T(8,128)} %shift_hbm.1, f32[1,128]{1,0:T(1,128)} %bitcast.13, ...), custom_call_target="tpu_custom_call" | custom-call | tf_op jit(solution)/shard_map/layer/pallas_call | solution.py:672
  65.0 0.0 copy-start
  65.0 1.6 %copy.22 = bf16[48,2048]{1,0:T(8,128)(2,1)} copy(bf16[48,2048]{1,0:T(8,128)(2,1)} %get-tuple-element.4) | data formatting | bytes 393216
  66.6 0.0 copy-done
  66.6 0.6 copy.23
Async XLA Ops:
  65.0 1.6 %copy-start = (f32[1,2,384]{2,1,0:T(2,128)S(1)}, f32[1,2,384]{2,1,0:T(2,128)}, u32[]{:S(2)}) copy-start(f32[1,2,384]{2,1,0:T(2,128)} %get-tuple-element.5) | copy-start | bytes 9220

commit v4 on v3

--- a/solution.py
+++ b/solution.py
@@ -315,6 +315,8 @@
         orecv,
         stsend,
         strecv,
+        joined,
+        weigh,
         gxsend,
         gxbuf,
         gzsend,
@@ -383,9 +385,8 @@
         w = wbuf[pl.ds(at, FEAT), :]
         gain = gain_ref[:, pl.ds(at, FEAT)]
 
-        @pl.loop(0, ROWS // 128)
-        def _(t):
-            rows = pl.ds(pl.multiple_of(t * 128, 128), 128)
+        for t in range(ROWS // 128):
+            rows = pl.ds(t * 128, 128)
             h = block[rows, :].astype(F32)
             squares = h[:, :128] * h[:, :128] + h[:, 128:] * h[:, 128:]
             product = dot((h * gain).astype(BF16), w)
@@ -516,10 +517,10 @@
             attend_all(kbuf.at[slot], vbuf.at[slot], False)
 
     attend_all(k_ref, vt_ref, True)
+    keys = pass_on(kbuf, keys, 2, key_all, key_all)
     attend(0, z >= 1)
-    keys = pass_on(kbuf, keys, 2, key_all, key_all)
+    values = pass_on(vbuf, values, 2, value_all, value_all)
     attend(3, z >= NZ - 1)
-    values = pass_on(vbuf, values, 2, value_all, value_all)
 
     for copy in gx_copies:
         copy.wait_recv()
@@ -534,10 +535,10 @@
     gzsend[...] = share
     gzbuf[z] = share
 
+    keys = pass_on(kbuf, keys, 3, pl.ds(0, HALF), pl.ds(HALF, HALF))
     attend(1, z >= 2)
-    keys = pass_on(kbuf, keys, 3, pl.ds(0, HALF), pl.ds(HALF, HALF))
+    values = pass_on(vbuf, values, 3, pl.ds(0, HD), pl.ds(HD, HD))
     attend(4, z >= NZ - 2)
-    values = pass_on(vbuf, values, 3, pl.ds(0, HD), pl.ds(HD, HD))
     attend(2, z >= 3)
     attend(5, z >= NZ - 3)
     for copy in (*keys, *values):
@@ -545,19 +546,32 @@
     gz_copies = [send(gzsend, gzbuf.at[z], place) for place in z_others]
     attend(6, z >= 4)
 
-    def partial_out(j):
-        total = jnp.maximum(low[j, 0:1, :], TINY)
-        return acc[j] * (1.0 / total), top[j, 0:1, :] + jnp.log2(total)
+    totals = jnp.maximum(jnp.concatenate([low[j, 0:1, :] for j in range(NX)], 0), TINY)
+    level = jnp.concatenate([top[j, 0:1, :] for j in range(NX)], 0) + jnp.log2(totals)
+    stsend[...] = level
+    st_copies = [send(stsend, strecv.at[n], {"x": x_others[n]}) for n in (1, 0, 2)]
+    for copy in st_copies:
+        copy.wait_recv()
+    theirs = [strecv[n] for n in range(3)]
+    highest = functools.reduce(jnp.maximum, theirs, level)
+    whole = sum((jnp.exp2(one - highest) for one in theirs), jnp.exp2(level - highest))
+    joint = highest + jnp.log2(whole)
+    joined[...] = joint
+    weigh[...] = jnp.exp2(level - joint) / totals
+
+    def contribution(j):
+        w = weigh[pl.ds(j, 1), :]
+        part = acc[j]
+        return part[:, :ROWS] * w[:, :ROWS] - part[:, ROWS:] * (lam_ref[0] * w[:, ROWS:])
 
     o_copies = []
     for n in (1, 0, 2):
-        j = x_others[n]
-        out, level = partial_out(j)
-        osend[n] = out.astype(BF16)
-        stsend[n] = jnp.broadcast_to(level, (8, 2 * ROWS))
-        o_copies.append(send(osend.at[n], orecv.at[n], {"x": j}))
-        o_copies.append(send(stsend.at[n], strecv.at[n], {"x": j}))
-    own_out, own_level = partial_out(x)
+        osend[n] = contribution(x_others[n]).astype(BF16)
+        o_copies.append(send(osend.at[n], orecv.at[n], {"x": x_others[n]}))
+    head_out = contribution(x)
+    sums = joined[pl.ds(x, 1), :] * LN2
+    sums_ref[0, 0:1, :] = sums[:, :ROWS]
+    sums_ref[0, 1:2, :] = sums[:, ROWS:]
 
     for copy in gz_copies:
         copy.wait_recv()
@@ -581,17 +595,8 @@
 
     for copy in o_copies:
         copy.wait_recv()
-    levels = [own_level] + [strecv[n, 0:1, :] for n in range(3)]
-    highest = functools.reduce(jnp.maximum, levels)
-    shares = [jnp.exp2(level - highest) for level in levels]
-    share_sum = sum(shares)
-    map_out = own_out * (shares[0] / share_sum)
     for n in range(3):
-        map_out = map_out + orecv[n].astype(F32) * (shares[n + 1] / share_sum)
-    sums = (highest + jnp.log2(share_sum)) * LN2
-    sums_ref[0, 0:1, :] = sums[:, :ROWS]
-    sums_ref[0, 1:2, :] = sums[:, ROWS:]
-    head_out = map_out[:, :ROWS] - lam_ref[0] * map_out[:, ROWS:]
+        head_out = head_out + orecv[n].astype(F32)
     head_out = head_out * lax.rsqrt(
         jnp.mean(head_out * head_out, axis=0, keepdims=True) + HEAD_EPS
     )
@@ -703,10 +708,12 @@
             VMEM((NX, 128, 2 * ROWS), F32),
             VMEM((NX, 8, 2 * ROWS), F32),
             VMEM((NX, 8, 2 * ROWS), F32),
-            VMEM((3, 128, 2 * ROWS), BF16),
-            VMEM((3, 128, 2 * ROWS), BF16),
-            VMEM((3, 8, 2 * ROWS), F32),
-            VMEM((3, 8, 2 * ROWS), F32),
+            VMEM((3, 128, ROWS), BF16),
+            VMEM((3, 128, ROWS), BF16),
+            VMEM((NX, 2 * ROWS), F32),
+            VMEM((3, NX, 2 * ROWS), F32),
+            VMEM((NX, 2 * ROWS), F32),
+            VMEM((NX, 2 * ROWS), F32),
             VMEM((HD, 256), F32),
             VMEM((NX, HD, 256), F32),
             VMEM((HD, 256), BF16),

time: 67.3 us -> 65.8 us (0.978)
  Pallas kernels: 63.7 us -> 62.2 us
    pallas_call x1, Pallas kernels: 63.7 us -> 62.2 us  [run_layer(): pl.pallas_call(layer, out_shape=(jax.ShapeDtypeStruct((share, D), BF16),...]
where the time goes in v4:
time: 65.8 us; the launch traced here: 65.7 us
  Pallas kernels  62.2 us (95%)
  local copies, waits for them, and re-layouts  2.2 us (3%)
  between operations  1.3 us (2%)
    pallas_call x1, Pallas kernels, run_layer(): pl.pallas_call(layer, out_shape=(jax.ShapeDtypeStruct((share, D), BF16),...  62.2 us
    unnamed x4, local copies, waits for them, and re-layouts  2.2 us

profile of v4, /device:TPU:1, one launch (start us, length us, event | category | flops | bytes accessed | tf_op | source)
XLA Modules:
  0.0 65.7 jit_solution(11466882065378181924)
XLA Ops:
  1.3 62.2 %layer.1 = (bf16[48,2048]{1,0:T(8,128)(2,1)}, f32[1,2,384]{2,1,0:T(2,128)}) custom-call(f32[1]{0:T(128)S(6)} %copy.21.lam_ref, bf16[384,256]{1,0:T(8,128)(2,1)} %hid_hbm.1, f32[1,2048]{1,0:T(1,128)} %bitcast.10, bf16[128,128]{1,0:T(8,128)(2,1)} %up_hbm.1, f32[1,128]{1,0:T(1,128)} %bitcast.12, f32[384,128]{1,0:T(8,128)} %shift_hbm.1, f32[1,128]{1,0:T(1,128)} %bitcast.13, ...), custom_call_target="tpu_custom_call" | custom-call | tf_op jit(solution)/shard_map/layer/pallas_call | solution.py:677
  63.5 0.0 copy-start
  63.5 1.6 %copy.22 = bf16[48,2048]{1,0:T(8,128)(2,1)} copy(bf16[48,2048]{1,0:T(8,128)(2,1)} %get-tuple-element.4) | data formatting | bytes 393216
  65.1 0.0 copy-done
  65.1 0.6 copy.23
Async XLA Ops:
  63.5 1.6 %copy-start = (f32[1,2,384]{2,1,0:T(2,128)S(1)}, f32[1,2,384]{2,1,0:T(2,128)}, u32[]{:S(2)}) copy-start(f32[1,2,384]{2,1,0:T(2,128)} %get-tuple-element.5) | copy-start | bytes 9220

commit v5 on v4

--- a/solution.py
+++ b/solution.py
@@ -253,11 +253,15 @@
     def __init__(self, ssem, rsem):
         self.ssem, self.rsem, self.copies = ssem, rsem, []
 
-    def send(self, src, dst, where):
+    def make(self, src, dst, where):
         n = len(self.copies)
         copy = remote(src, dst, self.ssem.at[n], self.rsem.at[n], where)
+        self.copies.append(copy)
+        return copy
+
+    def send(self, src, dst, where):
+        copy = self.make(src, dst, where)
         copy.start()
-        self.copies.append(copy)
         return copy
 
 
@@ -323,6 +327,7 @@
         gzbuf,
         reads,
         local,
+        state_ref,
         mix_ref,
         psend,
         precv,
@@ -434,10 +439,25 @@
     q_ref[...] = (proj[:, 512:640] * (scale * (LOG2E * HD**-0.5))).astype(BF16)
 
     def pass_on(buf, source, slot, first, second):
-        source[0].wait_recv()
-        ahead = send(buf.at[slot - 1, first], buf.at[slot if slot < 3 else 6, first], z_up)
-        source[1].wait_recv()
-        back = send(buf.at[slot + 2, second], buf.at[slot + 3, second], z_down)
+        ahead = courier.make(
+            buf.at[slot - 1, first], buf.at[slot if slot < 3 else 6, first], z_up
+        )
+        back = courier.make(buf.at[slot + 2, second], buf.at[slot + 3, second], z_down)
+
+        def forth(n, copy):
+            source[n].wait_recv()
+            copy.start()
+
+        @pl.when(z < 3)
+        def _():
+            forth(1, back)
+            forth(0, ahead)
+
+        @pl.when(z >= 3)
+        def _():
+            forth(0, ahead)
+            forth(1, back)
+
         return ahead, back
 
     key_all, value_all = pl.ds(0, ROWS), pl.ds(0, 128)
@@ -475,18 +495,24 @@
         qwide[j] = by_head(qbuf[j])
     tiles = [slice(t * 256, (t + 1) * 256) for t in range(3)]
 
-    def attend_all(k_block, v_block, own):
-        k_all, v_all = k_block[...], v_block[...]
+    def attend_all(blocks, own):
+        k_all = [k_block[...] for k_block, _ in blocks]
+        v_all = jnp.concatenate([v_block[...] for _, v_block in blocks], 1)
 
         def scores_of(j):
-            found = [dot_nt(k_all, qwide[j, cols, :]) for cols in tiles]
+            found = [[dot_nt(k, qwide[j, cols, :]) for k in k_all] for cols in tiles]
             if own:
                 for t in range(3):
                     key_at = iota((ROWS, 256), 0)
                     query_at = lax.rem(iota((ROWS, 256), 1) + t * 256, ROWS)
                     keep = query_at - key_at >= (x - j) * ROWS
-                    found[t] = jnp.where(keep, found[t], NEGATIVE)
-            return found, [jnp.max(s, axis=0, keepdims=True) for s in found]
+                    found[t] = [jnp.where(keep, s, NEGATIVE) for s in found[t]]
+            return found, [
+                functools.reduce(
+                    jnp.maximum, [jnp.max(s, axis=0, keepdims=True) for s in group]
+                )
+                for group in found
+            ]
 
         ready = scores_of(0)
         for j in range(NX):
@@ -498,9 +524,9 @@
                 totals = [acc[j, :, cols] for cols in tiles]
             for t, cols in enumerate(tiles):
                 new = highest[t] if own else jnp.maximum(olds[t], highest[t])
-                weights = jnp.exp2(scores[t] - new)
-                part = jnp.sum(weights, axis=0, keepdims=True)
-                seen = dot(v_all, weights.astype(BF16))
+                weights = [jnp.exp2(s - new) for s in scores[t]]
+                part = sum(jnp.sum(w, axis=0, keepdims=True) for w in weights)
+                seen = dot(v_all, jnp.concatenate([w.astype(BF16) for w in weights], 0))
                 top[j, 0:1, cols] = new
                 if own:
                     low[j, 0:1, cols] = part
@@ -511,16 +537,16 @@
                     acc[j, :, cols] = totals[t] * rescale + seen
             ready = following
 
-    def attend(slot, needed):
+    def attend(slots, needed):
         @pl.when(needed)
         def _():
-            attend_all(kbuf.at[slot], vbuf.at[slot], False)
-
-    attend_all(k_ref, vt_ref, True)
+            attend_all([(kbuf.at[slot], vbuf.at[slot]) for slot in slots], False)
+
+    attend_all([(k_ref, vt_ref)], True)
     keys = pass_on(kbuf, keys, 2, key_all, key_all)
-    attend(0, z >= 1)
+    attend([0, 3], z == NZ - 1)
+    attend([0], (z >= 1) & (z < NZ - 1))
     values = pass_on(vbuf, values, 2, value_all, value_all)
-    attend(3, z >= NZ - 1)
 
     for copy in gx_copies:
         copy.wait_recv()
@@ -536,20 +562,41 @@
     gzbuf[z] = share
 
     keys = pass_on(kbuf, keys, 3, pl.ds(0, HALF), pl.ds(HALF, HALF))
-    attend(1, z >= 2)
+    attend([1, 4], z >= NZ - 2)
+    attend([1], (z >= 2) & (z < NZ - 2))
     values = pass_on(vbuf, values, 3, pl.ds(0, HD), pl.ds(HD, HD))
-    attend(4, z >= NZ - 2)
-    attend(2, z >= 3)
-    attend(5, z >= NZ - 3)
-    for copy in (*keys, *values):
-        copy.wait_recv()
-    gz_copies = [send(gzsend, gzbuf.at[z], place) for place in z_others]
-    attend(6, z >= 4)
+    attend([2, 5], z >= NZ - 3)
+    attend([2], (z >= 3) & (z < NZ - 3))
+    gz_copies = []
+    for n in range(1, NZ):
+        at = 50 + n
+        gz_copies.append(
+            remote(gzsend, gzbuf.at[z], ssem.at[at], rsem.at[at], {"z": lax.rem(z + n, NZ)})
+        )
+
+    def finish_ring():
+        for copy in (*keys, *values):
+            copy.wait_recv()
+        for n in range(1, NZ):
+
+            @pl.when(z + n < NZ)
+            def _(n=n):
+                gz_copies[n - 1].start()
+
+    @pl.when(z >= 4)
+    def _():
+        finish_ring()
+        attend_all([(kbuf.at[6], vbuf.at[6])], False)
 
     totals = jnp.maximum(jnp.concatenate([low[j, 0:1, :] for j in range(NX)], 0), TINY)
     level = jnp.concatenate([top[j, 0:1, :] for j in range(NX)], 0) + jnp.log2(totals)
     stsend[...] = level
     st_copies = [send(stsend, strecv.at[n], {"x": x_others[n]}) for n in (1, 0, 2)]
+
+    @pl.when(z < 4)
+    def _():
+        finish_ring()
+
     for copy in st_copies:
         copy.wait_recv()
     theirs = [strecv[n] for n in range(3)]
@@ -573,14 +620,21 @@
     sums_ref[0, 0:1, :] = sums[:, :ROWS]
     sums_ref[0, 1:2, :] = sums[:, ROWS:]
 
-    for copy in gz_copies:
-        copy.wait_recv()
-    state = none
+    for n in range(1, NZ):
+
+        @pl.when(z >= n)
+        def _(n=n):
+            gz_copies[n - 1].wait_recv()
+
+    state_ref[...] = none
     for n in range(NZ - 1):
-        step = unpacked(gzbuf[n].astype(F32) + packed_identity())
-        after = fine_dot(step[:, :128], state) + step[:, 128:]
-        state = jnp.where(n < z, after, state)
-    state = fine_dot(before_x[:, :128], state) + before_x[:, 128:]
+
+        @pl.when(n < z)
+        def _(n=n):
+            step = unpacked(gzbuf[n].astype(F32) + packed_identity())
+            state_ref[...] = fine_dot(step[:, :128], state_ref[...]) + step[:, 128:]
+
+    state = fine_dot(before_x[:, :128], state_ref[...]) + before_x[:, 128:]
     recurrent = local[...] + fine_dot(reads[...], state)
     first = iota((ROWS, 128), 1) < HD
 
@@ -666,13 +720,18 @@
     out_ref[:, two] = (right_half * scale * out_gain_ref[:, two]).astype(BF16)
     for copy in courier.copies:
         copy.wait_send()
+    for n in range(1, NZ):
+
+        @pl.when(z + n < NZ)
+        def _(n=n):
+            gz_copies[n - 1].wait_send()
 
 
 def run_layer(lam, hid, gain, up, base, shift, rate, wr, wa, out_gain, weights):
     whole = pl.BlockSpec(memory_space=VMEM)
     far = pl.BlockSpec(memory_space=pl.ANY)
     share = ROWS // (NY * NC)
-    count = 13 + 16 + 3 + 3 + 7 + 6 + 10
+    count = 13 + 16 + 3 + 3 + 3 + 3 + 10 + 7
     rows = VMEM((ROWS, 128), BF16)
     return pl.pallas_call(
         layer,
@@ -720,6 +779,7 @@
             VMEM((NZ, HD, 256), BF16),
             VMEM((ROWS, 128), F32),
             VMEM((ROWS, 128), F32),
+            VMEM((128, 128), F32),
             VMEM((ROWS, 256), BF16),
             VMEM((4 * share, D), BF16),
             VMEM((4 * share, D), BF16),

time: 65.8 us -> 62.6 us (0.951)
  Pallas kernels: 62.2 us -> 59 us
    pallas_call x1, Pallas kernels: 62.2 us -> 59 us  [run_layer(): pl.pallas_call(layer, out_shape=(jax.ShapeDtypeStruct((share, D), BF16),...]
where the time goes in v5:
time: 62.6 us; the launch traced here: 62.5 us
  Pallas kernels  59 us (94%)
  local copies, waits for them, and re-layouts  2.2 us (4%)
  between operations  1.3 us (2%)
    pallas_call x1, Pallas kernels, run_layer(): pl.pallas_call(layer, out_shape=(jax.ShapeDtypeStruct((share, D), BF16),...  59 us
    unnamed x4, local copies, waits for them, and re-layouts  2.2 us

profile of v5, /device:TPU:1, one launch (start us, length us, event | category | flops | bytes accessed | tf_op | source)
XLA Modules:
  0.0 62.5 jit_solution(4235594201883785970)
XLA Ops:
  1.3 59.0 %layer.1 = (bf16[48,2048]{1,0:T(8,128)(2,1)}, f32[1,2,384]{2,1,0:T(2,128)}) custom-call(f32[1]{0:T(128)S(6)} %copy.21.lam_ref, bf16[384,256]{1,0:T(8,128)(2,1)} %hid_hbm.1, f32[1,2048]{1,0:T(1,128)} %bitcast.10, bf16[128,128]{1,0:T(8,128)(2,1)} %up_hbm.1, f32[1,128]{1,0:T(1,128)} %bitcast.12, f32[384,128]{1,0:T(8,128)} %shift_hbm.1, f32[1,128]{1,0:T(1,128)} %bitcast.13, ...), custom_call_target="tpu_custom_call" | custom-call | tf_op jit(solution)/shard_map/layer/pallas_call | solution.py:736
  60.3 0.0 copy-start
  60.3 1.6 %copy.22 = bf16[48,2048]{1,0:T(8,128)(2,1)} copy(bf16[48,2048]{1,0:T(8,128)(2,1)} %get-tuple-element.4) | data formatting | bytes 393216
  61.9 0.0 copy-done
  61.9 0.6 copy.23
Async XLA Ops:
  60.3 1.6 %copy-start = (f32[1,2,384]{2,1,0:T(2,128)S(1)}, f32[1,2,384]{2,1,0:T(2,128)}, u32[]{:S(2)}) copy-start(f32[1,2,384]{2,1,0:T(2,128)} %get-tuple-element.5) | copy-start | bytes 9220

commit v6 on v5

--- a/solution.py
+++ b/solution.py
@@ -384,10 +384,10 @@
     for load in loads[1:]:
         load.wait()
 
-    def add(number, fresh=False):
+    def add(number, fresh=False, cols=slice(0, 896), squared=True):
         block = hbuf.at[number]
         at = pl.multiple_of(number * FEAT, FEAT)
-        w = wbuf[pl.ds(at, FEAT), :]
+        w = wbuf[pl.ds(at, FEAT), cols]
         gain = gain_ref[:, pl.ds(at, FEAT)]
 
         for t in range(ROWS // 128):
@@ -399,8 +399,9 @@
                 sumsq[rows, :] = squares
                 proj[rows, :] = product
             else:
-                sumsq[rows, :] += squares
-                proj[rows, :] += product
+                if squared:
+                    sumsq[rows, :] += squares
+                proj[rows, cols] += product
 
     add(own, True)
     beside.wait_recv()
@@ -430,7 +431,7 @@
     add(far)
     relays[4].wait_recv()
     relays[5].wait_recv()
-    add(across * 2 + other)
+    add(across * 2 + other, cols=slice(512, 896))
 
     total = jnp.sum(sumsq[...], axis=1, keepdims=True)
     scale = lax.rsqrt(total * (1.0 / D) + NORM_EPS)
@@ -464,6 +465,8 @@
     keys = (send(k_ref, kbuf.at[0], z_up), send(k_ref, kbuf.at[3], z_down))
     values = (send(vt_ref, vbuf.at[0], z_up), send(vt_ref, vbuf.at[3], z_down))
     q_copies = [send(q_ref, qbuf.at[x], {"x": x_others[n]}) for n in (1, 0, 2)]
+
+    add(across * 2 + other, cols=slice(0, 512), squared=False)
 
     @pl.loop(0, ROWS // 128)
     def _(t):

time: 62.6 us -> 62.5 us (level)
  no operation moved by 1% of the time
where the time goes in v6:
time: 62.5 us; the launch traced here: 62.4 us
  Pallas kernels  58.9 us (94%)
  local copies, waits for them, and re-layouts  2.2 us (4%)
  between operations  1.3 us (2%)
    pallas_call x1, Pallas kernels, run_layer(): pl.pallas_call(layer, out_shape=(jax.ShapeDtypeStruct((share, D), BF16),...  58.9 us
    unnamed x4, local copies, waits for them, and re-layouts  2.2 us

profile of v6, /device:TPU:1, one launch (start us, length us, event | category | flops | bytes accessed | tf_op | source)
XLA Modules:
  0.0 62.4 jit_solution(1907604795014338719)
XLA Ops:
  1.3 58.9 %layer.1 = (bf16[48,2048]{1,0:T(8,128)(2,1)}, f32[1,2,384]{2,1,0:T(2,128)}) custom-call(f32[1]{0:T(128)S(6)} %copy.21.lam_ref, bf16[384,256]{1,0:T(8,128)(2,1)} %hid_hbm.1, f32[1,2048]{1,0:T(1,128)} %bitcast.10, bf16[128,128]{1,0:T(8,128)(2,1)} %up_hbm.1, f32[1,128]{1,0:T(1,128)} %bitcast.12, f32[384,128]{1,0:T(8,128)} %shift_hbm.1, f32[1,128]{1,0:T(1,128)} %bitcast.13, ...), custom_call_target="tpu_custom_call" | custom-call | tf_op jit(solution)/shard_map/layer/pallas_call | solution.py:739
  60.2 0.0 copy-start
  60.2 1.6 %copy.22 = bf16[48,2048]{1,0:T(8,128)(2,1)} copy(bf16[48,2048]{1,0:T(8,128)(2,1)} %get-tuple-element.4) | data formatting | bytes 393216
  61.8 0.0 copy-done
  61.8 0.6 copy.23
Async XLA Ops:
  60.2 1.6 %copy-start = (f32[1,2,384]{2,1,0:T(2,128)S(1)}, f32[1,2,384]{2,1,0:T(2,128)}, u32[]{:S(2)}) copy-start(f32[1,2,384]{2,1,0:T(2,128)} %get-tuple-element.5) | copy-start | bytes 9220
